TPU v7x, 512 devices: a whole 4x8x8 slice. The times are simulated.
512 devices in a mesh: sp: 64 (over z, y), tp: 8 (over x, core).
Axes of the slice: x: 4, y: 8, z: 8, core: 2. Of those that a mesh axis runs over, the one named last changes fastest.
Arguments:
- queries: bfloat16 [16384, 512], P('sp', 'tp'), may hold values from -8 to 8
- keys: bfloat16 [16384, 512], P('sp', 'tp'), may hold values from -8 to 8
- values: bfloat16 [16384, 512], P('sp', 'tp'), may hold values from -6 to 6
- score_shift: float32 [8], P('tp'), may hold values from 3 to 20
- resid: bfloat16 [16384, 2048], P(('sp', 'tp')), may hold values from -6 to 6
- w_out: bfloat16 [512, 2048], replicated, may hold values from -0.25 to 0.25
- gain_mix: float32 [2048], replicated, may hold values from 0.1 to 1.9
- gain_pre: float32 [2048], replicated, may hold values from 0.1 to 1.9
- w_gate: bfloat16 [2048, 5632], P('sp', 'tp'), may hold values from -0.125 to 0.125
- w_up: bfloat16 [2048, 5632], P('sp', 'tp'), may hold values from -0.125 to 0.125
- conv_gate: float32 [3, 5632], P(None, 'tp'), may hold values from -3 to 3
- conv_up: float32 [3, 5632], P(None, 'tp'), may hold values from -3 to 3
- w_down: bfloat16 [5632, 2048], P('tp', 'sp'), may hold values from -0.078125 to 0.078125
- gain_post: float32 [2048], replicated, may hold values from 0.1 to 1.9
Outputs:
- result: bfloat16 [16384, 2048], P(('sp', 'tp'))
All inputs are finite; a program needn't handle non-finite values.
Results may differ from a plain program's by a relative error of at most 0.017.
Values may be sent and summed in bfloat16 or wider, within the bound.
A program may use at most 64 MiB of HBM per device.

v0:
```python
import jax
import jax.numpy as jnp
from jax import lax
from jax.sharding import PartitionSpec as P

HEAD_DIM = 64
KERNEL = 3


def side_by_side(arrays, axis, dim, along):
    widths = [a.shape[along] for a in arrays]
    both = jnp.concatenate(arrays, axis=along)
    out = lax.all_gather(both, axis, axis=dim, tiled=True)
    return tuple(jnp.split(out, [sum(widths[:k]) for k in range(1, len(widths))], axis=along))


def laid_out(parts, dim):
    parts = jnp.moveaxis(parts, 0, dim)
    lengths = parts.shape
    return parts.reshape(*lengths[:dim], lengths[dim] * lengths[dim + 1], *lengths[dim + 2 :])


def from_everyone(x, axis):
    length = lax.axis_size(axis)
    return lax.all_to_all(jnp.broadcast_to(x[None], (length, *x.shape)), axis, 0, 0, tiled=True)


def gathered_copies(x, axis, dim):
    return laid_out(from_everyone(x, axis), dim)


def from_behind(x, axis, by):
    length = lax.axis_size(axis)
    pairs = [(i, i + by) for i in range(length) if 0 <= i + by < length]
    return lax.ppermute(x, axis, pairs)


def split_up(x, dim, length):
    before, after = (x.shape[:dim], x.shape[dim + 1 :])
    return jnp.moveaxis(x.reshape(*before, length, -1, *after), dim, 0)


def sum_at_owner(x, axis, dim):
    parts = split_up(x, dim, lax.axis_size(axis))
    arrived = lax.all_to_all(parts, axis, split_axis=0, concat_axis=0, tiled=True)
    return arrived.astype(jnp.float32).sum(axis=0)


def rms_scale(values_in):
    return values_in * lax.rsqrt(jnp.mean(values_in * values_in, axis=-1, keepdims=True) + 1e-06)


def collect_weights(w_gate, w_up, w_down):
    gate_whole, up_whole = side_by_side((w_gate, w_up), "sp", 0, 1)
    down_whole = lax.all_gather(w_down, "sp", axis=1, tiled=True)
    return (gate_whole, up_whole, down_whole)


def stick_attention(queries, key_whole, value_whole, score_shift):
    tok_rows = queries.shape[0]
    local_heads = queries.shape[1] // HEAD_DIM
    total = key_whole.shape[0]
    shards = total // tok_rows
    group = max(
        (
            factor
            for factor in range(1, shards + 1)
            if shards % factor == 0 and factor * tok_rows <= max(2048, tok_rows)
        )
    )
    span = group * tok_rows
    offset = lax.axis_index("sp") * tok_rows
    query_heads = queries.reshape(tok_rows, local_heads, HEAD_DIM)
    key_heads = key_whole.reshape(total, local_heads, HEAD_DIM)
    value_heads = value_whole.reshape(total, local_heads, HEAD_DIM)
    query_pos = offset + jnp.arange(tok_rows, dtype=jnp.int32)
    last_block = (offset + tok_rows - 1) // span

    def visit(turn, carry):
        accum, tail = carry
        block_start = (last_block - turn) * span
        key_block = lax.dynamic_slice_in_dim(key_heads, block_start, span, 0)
        value_block = lax.dynamic_slice_in_dim(value_heads, block_start, span, 0)
        scores = jnp.einsum(
            "qhd,khd->hqk", query_heads, key_block, preferred_element_type=jnp.float32
        )
        scores = scores * HEAD_DIM ** (-0.5) - score_shift[:, None, None]
        key_pos = block_start + jnp.arange(span, dtype=jnp.int32)
        causal = (key_pos[None, :] < query_pos[:, None])[None, :, :]
        log_keep = jnp.where(causal, -jax.nn.softplus(scores), 0.0)
        later = lax.cumsum(log_keep, axis=2, reverse=True) - log_keep
        weights = jnp.where(
            causal, jnp.exp(jax.nn.log_sigmoid(scores) + later + tail[:, :, None]), 0.0
        ).astype(jnp.bfloat16)
        accum = accum + jnp.einsum(
            "hqk,khd->hqd", weights, value_block, preferred_element_type=jnp.float32
        )
        return (accum, tail + jnp.sum(log_keep, axis=2))

    start_carry = (
        jnp.zeros((local_heads, tok_rows, HEAD_DIM), jnp.float32),
        jnp.zeros((local_heads, tok_rows), jnp.float32),
    )
    accum, _ = lax.fori_loop(0, last_block + 1, visit, start_carry)
    return accum.transpose(1, 0, 2).reshape(tok_rows, local_heads * HEAD_DIM).astype(jnp.bfloat16)


def local(
    queries,
    keys,
    values,
    score_shift,
    resid,
    w_out,
    gain_mix,
    gain_pre,
    w_gate,
    w_up,
    conv_gate,
    conv_up,
    w_down,
    gain_post,
):
    gate_whole, up_whole, down_whole = collect_weights(w_gate, w_up, w_down)
    key_whole, value_whole = side_by_side((keys, values), "sp", 0, 1)
    attended = stick_attention(queries, key_whole, value_whole, score_shift)
    head_rows = lax.all_to_all(attended, "tp", split_axis=0, concat_axis=1, tiled=True)
    mixed = jnp.dot(head_rows, w_out, preferred_element_type=jnp.float32).astype(jnp.bfloat16)
    middle = (resid.astype(jnp.float32) + gain_mix * rms_scale(mixed.astype(jnp.float32))).astype(
        jnp.bfloat16
    )
    normed = (gain_pre * rms_scale(middle.astype(jnp.float32))).astype(jnp.bfloat16)
    piece = gathered_copies(normed, "tp", 0)
    gate_part = jnp.dot(piece, gate_whole, preferred_element_type=jnp.float32).astype(jnp.bfloat16)
    up_part = jnp.dot(piece, up_whole, preferred_element_type=jnp.float32).astype(jnp.bfloat16)
    projected = jnp.concatenate([gate_part, up_part], axis=1)
    tok_rows = projected.shape[0]
    local_units = projected.shape[1] // 2
    edge = from_behind(projected[tok_rows - (KERNEL - 1) :], "sp", 1)
    extended = jnp.concatenate([edge, projected], axis=0).astype(jnp.float32)
    taps = jnp.concatenate([conv_gate, conv_up], axis=1)
    convolved = taps[0] * extended[0:tok_rows]
    for tap in range(1, KERNEL):
        convolved = convolved + taps[tap] * extended[tap : tap + tok_rows]
    hidden = (jax.nn.silu(convolved[:, :local_units]) * convolved[:, local_units:]).astype(
        jnp.bfloat16
    )
    summed = sum_at_owner(
        jnp.dot(hidden, down_whole, preferred_element_type=jnp.float32).astype(jnp.bfloat16),
        "tp",
        0,
    )
    ffn_out = summed.astype(jnp.bfloat16)
    return (middle.astype(jnp.float32) + gain_post * rms_scale(ffn_out.astype(jnp.float32))).astype(
        jnp.bfloat16
    )


def solution(mesh):
    in_specs = (
        P("sp", "tp"),
        P("sp", "tp"),
        P("sp", "tp"),
        P("tp"),
        P(("sp", "tp"), None),
        P(),
        P(),
        P(),
        P("sp", "tp"),
        P("sp", "tp"),
        P(None, "tp"),
        P(None, "tp"),
        P("tp", "sp"),
        P(),
    )
    out_specs = P(("sp", "tp"), None)
    return jax.shard_map(local, mesh=mesh, in_specs=in_specs, out_specs=out_specs, check_vma=False)
```

profile of v0, /device:TPU:448, one launch (start us, length us, event | category | flops | bytes accessed | tf_op | source)
XLA Modules:
  0.0 331.4 jit_solution(313989612567962187)
XLA Ops:
  10.5 88.7 %all-gather.4.cloned.1.call-done = bf16[16384,128]{0,1:T(8,128)(2,1)} async-done(((bf16[256,128]{0,1:T(8,128)(2,1)}), bf16[16384,128]{0,1:T(8,128)(2,1)}) %all-gather.4.cloned.1.call-update) | async-done | bytes 4194320 | tf_op jit(solution)/shard_map/all_gather | solution.py:13
  99.2 4.5 %slice_bitcast_fusion.2 = (bf16[16384,1,64]{0,2,1:T(8,128)(2,1)}, bf16[16384,1,64]{0,2,1:T(8,128)(2,1)}) fusion(bf16[16384,128]{0,1:T(8,128)(2,1)} %all-gather.4.cloned.1.call-done), kind=kLoop, calls=%fused_computation.39 | loop fusion | bytes 8388608 | tf_op jit(solution)/shard_map/reshape | solution.py:75
  103.8 146.1 %while.13 = (s32[]{:T(128)}, f32[1,256,64]{1,2,0:T(8,128)S(1)}, f32[1,256]{1,0:T(1,128)S(1)}, s32[]{:T(128)}, s32[]{:T(128)}, /*index=5*/bf16[16384,1,64]{0,2,1:...) while((s32[]{:T(128)}, f32[1,256,64]{1,2,0:T(8,128)S(1)}, ...), condition=%wide.region_4.5_spmd.clone, body=%wide.region_0.4_spmd.clone.sunk | while | flops 219236352 | bytes 19711708 | solution.py:104
  103.8 4.6 %fusion.62 = (f32[256]{0:T(256)S(1)}, f32[256,2048]{0,1:T(8,128)S(1)}, f32[256,2048]{0,1:T(8,128)}) fusion(s32[256]{0:T(256)S(1)} %iota_add_fusion.4, s32[2048]{0:T(1024)S(1)} %iota_add_fusion.5, f32[]{:T(128)} %bitcast.72, bf16[256,1,64]{0,2,1:T(8,128)(2,1)S(1)} %get-tuple-element.219, bf16[16384,1,64]{0,2,1:T(8,128)(2,1)} %get-tuple-element.218, ...), kind=kOutput, calls=%fused_computation.31.clone.1 | convolution fusion | flops 73400064 | bytes 4499972 | tf_op jit(solution)/shard_map/while/body/qhd,khd->hqk/dot_general | solution.py:84
  108.4 5.0 %fusion.63 = f32[1,256,16,128]{1,2,3,0:T(8,128)S(1)} fusion(f32[1,256,16,128]{1,3,2,0:T(8,128)S(1)} %bitcast.76), kind=kOutput, calls=%fused_computation.16.clone.1 | output fusion | flops 66584576 | bytes 4194304 | tf_op jit(solution)/shard_map/reduce-window
  116.1 4.6 %fusion.64 = bf16[256,2048]{0,1:T(8,128)(2,1)S(1)} fusion(f32[1,256,16,128]{1,3,2,0:T(8,128)} %copy.29, f32[256,2048]{0,1:T(8,128)} %get-tuple-element.181, f32[256]{0:T(256)S(1)} %bitcast.82, f32[256,16]{0,1:T(8,128)S(1)} %slice_bitcast_fusion.7, s32[256]{0:T(256)S(1)} %iota_add_fusion.4, s32[2048]{0:T(1024)S(1)} %iota_add_fusion.5), kind=kLoop, calls=%fused_computation.8.clone.1 | loop fusion | flops 12058624 | bytes 5269504 | tf_op jit(solution)/shard_map/while/body/convert_element_type | solution.py:94
  122.1 4.6 %fusion.62 = (f32[256]{0:T(256)S(1)}, f32[256,2048]{0,1:T(8,128)S(1)}, f32[256,2048]{0,1:T(8,128)}) fusion(s32[256]{0:T(256)S(1)} %iota_add_fusion.4, s32[2048]{0:T(1024)S(1)} %iota_add_fusion.5, f32[]{:T(128)} %bitcast.72, bf16[256,1,64]{0,2,1:T(8,128)(2,1)S(1)} %get-tuple-element.219, bf16[16384,1,64]{0,2,1:T(8,128)(2,1)} %get-tuple-element.218, ...), kind=kOutput, calls=%fused_computation.31.clone.1 | convolution fusion | flops 73400064 | bytes 4499972 | tf_op jit(solution)/shard_map/while/body/qhd,khd->hqk/dot_general | solution.py:84
  126.6 5.0 %fusion.63 = f32[1,256,16,128]{1,2,3,0:T(8,128)S(1)} fusion(f32[1,256,16,128]{1,3,2,0:T(8,128)S(1)} %bitcast.76), kind=kOutput, calls=%fused_computation.16.clone.1 | output fusion | flops 66584576 | bytes 4194304 | tf_op jit(solution)/shard_map/reduce-window
  134.4 4.6 %fusion.64 = bf16[256,2048]{0,1:T(8,128)(2,1)S(1)} fusion(f32[1,256,16,128]{1,3,2,0:T(8,128)} %copy.29, f32[256,2048]{0,1:T(8,128)} %get-tuple-element.181, f32[256]{0:T(256)S(1)} %bitcast.82, f32[256,16]{0,1:T(8,128)S(1)} %slice_bitcast_fusion.7, s32[256]{0:T(256)S(1)} %iota_add_fusion.4, s32[2048]{0:T(1024)S(1)} %iota_add_fusion.5), kind=kLoop, calls=%fused_computation.8.clone.1 | loop fusion | flops 12058624 | bytes 5269504 | tf_op jit(solution)/shard_map/while/body/convert_element_type | solution.py:94
  140.3 4.6 %fusion.62 = (f32[256]{0:T(256)S(1)}, f32[256,2048]{0,1:T(8,128)S(1)}, f32[256,2048]{0,1:T(8,128)}) fusion(s32[256]{0:T(256)S(1)} %iota_add_fusion.4, s32[2048]{0:T(1024)S(1)} %iota_add_fusion.5, f32[]{:T(128)} %bitcast.72, bf16[256,1,64]{0,2,1:T(8,128)(2,1)S(1)} %get-tuple-element.219, bf16[16384,1,64]{0,2,1:T(8,128)(2,1)} %get-tuple-element.218, ...), kind=kOutput, calls=%fused_computation.31.clone.1 | convolution fusion | flops 73400064 | bytes 4499972 | tf_op jit(solution)/shard_map/while/body/qhd,khd->hqk/dot_general | solution.py:84
  144.9 5.0 %fusion.63 = f32[1,256,16,128]{1,2,3,0:T(8,128)S(1)} fusion(f32[1,256,16,128]{1,3,2,0:T(8,128)S(1)} %bitcast.76), kind=kOutput, calls=%fused_computation.16.clone.1 | output fusion | flops 66584576 | bytes 4194304 | tf_op jit(solution)/shard_map/reduce-window
  152.6 4.6 %fusion.64 = bf16[256,2048]{0,1:T(8,128)(2,1)S(1)} fusion(f32[1,256,16,128]{1,3,2,0:T(8,128)} %copy.29, f32[256,2048]{0,1:T(8,128)} %get-tuple-element.181, f32[256]{0:T(256)S(1)} %bitcast.82, f32[256,16]{0,1:T(8,128)S(1)} %slice_bitcast_fusion.7, s32[256]{0:T(256)S(1)} %iota_add_fusion.4, s32[2048]{0:T(1024)S(1)} %iota_add_fusion.5), kind=kLoop, calls=%fused_computation.8.clone.1 | loop fusion | flops 12058624 | bytes 5269504 | tf_op jit(solution)/shard_map/while/body/convert_element_type | solution.py:94
  158.6 4.6 %fusion.62 = (f32[256]{0:T(256)S(1)}, f32[256,2048]{0,1:T(8,128)S(1)}, f32[256,2048]{0,1:T(8,128)}) fusion(s32[256]{0:T(256)S(1)} %iota_add_fusion.4, s32[2048]{0:T(1024)S(1)} %iota_add_fusion.5, f32[]{:T(128)} %bitcast.72, bf16[256,1,64]{0,2,1:T(8,128)(2,1)S(1)} %get-tuple-element.219, bf16[16384,1,64]{0,2,1:T(8,128)(2,1)} %get-tuple-element.218, ...), kind=kOutput, calls=%fused_computation.31.clone.1 | convolution fusion | flops 73400064 | bytes 4499972 | tf_op jit(solution)/shard_map/while/body/qhd,khd->hqk/dot_general | solution.py:84
  163.1 5.0 %fusion.63 = f32[1,256,16,128]{1,2,3,0:T(8,128)S(1)} fusion(f32[1,256,16,128]{1,3,2,0:T(8,128)S(1)} %bitcast.76), kind=kOutput, calls=%fused_computation.16.clone.1 | output fusion | flops 66584576 | bytes 4194304 | tf_op jit(solution)/shard_map/reduce-window
  170.9 4.7 %fusion.64 = bf16[256,2048]{0,1:T(8,128)(2,1)S(1)} fusion(f32[1,256,16,128]{1,3,2,0:T(8,128)} %copy.29, f32[256,2048]{0,1:T(8,128)} %get-tuple-element.181, f32[256]{0:T(256)S(1)} %bitcast.82, f32[256,16]{0,1:T(8,128)S(1)} %slice_bitcast_fusion.7, s32[256]{0:T(256)S(1)} %iota_add_fusion.4, s32[2048]{0:T(1024)S(1)} %iota_add_fusion.5), kind=kLoop, calls=%fused_computation.8.clone.1 | loop fusion | flops 12058624 | bytes 5269504 | tf_op jit(solution)/shard_map/while/body/convert_element_type | solution.py:94
  176.9 4.6 %fusion.62 = (f32[256]{0:T(256)S(1)}, f32[256,2048]{0,1:T(8,128)S(1)}, f32[256,2048]{0,1:T(8,128)}) fusion(s32[256]{0:T(256)S(1)} %iota_add_fusion.4, s32[2048]{0:T(1024)S(1)} %iota_add_fusion.5, f32[]{:T(128)} %bitcast.72, bf16[256,1,64]{0,2,1:T(8,128)(2,1)S(1)} %get-tuple-element.219, bf16[16384,1,64]{0,2,1:T(8,128)(2,1)} %get-tuple-element.218, ...), kind=kOutput, calls=%fused_computation.31.clone.1 | convolution fusion | flops 73400064 | bytes 4499972 | tf_op jit(solution)/shard_map/while/body/qhd,khd->hqk/dot_general | solution.py:84
  181.5 5.0 %fusion.63 = f32[1,256,16,128]{1,2,3,0:T(8,128)S(1)} fusion(f32[1,256,16,128]{1,3,2,0:T(8,128)S(1)} %bitcast.76), kind=kOutput, calls=%fused_computation.16.clone.1 | output fusion | flops 66584576 | bytes 4194304 | tf_op jit(solution)/shard_map/reduce-window
  189.2 4.6 %fusion.64 = bf16[256,2048]{0,1:T(8,128)(2,1)S(1)} fusion(f32[1,256,16,128]{1,3,2,0:T(8,128)} %copy.29, f32[256,2048]{0,1:T(8,128)} %get-tuple-element.181, f32[256]{0:T(256)S(1)} %bitcast.82, f32[256,16]{0,1:T(8,128)S(1)} %slice_bitcast_fusion.7, s32[256]{0:T(256)S(1)} %iota_add_fusion.4, s32[2048]{0:T(1024)S(1)} %iota_add_fusion.5), kind=kLoop, calls=%fused_computation.8.clone.1 | loop fusion | flops 12058624 | bytes 5269504 | tf_op jit(solution)/shard_map/while/body/convert_element_type | solution.py:94
  195.1 4.5 %fusion.62 = (f32[256]{0:T(256)S(1)}, f32[256,2048]{0,1:T(8,128)S(1)}, f32[256,2048]{0,1:T(8,128)}) fusion(s32[256]{0:T(256)S(1)} %iota_add_fusion.4, s32[2048]{0:T(1024)S(1)} %iota_add_fusion.5, f32[]{:T(128)} %bitcast.72, bf16[256,1,64]{0,2,1:T(8,128)(2,1)S(1)} %get-tuple-element.219, bf16[16384,1,64]{0,2,1:T(8,128)(2,1)} %get-tuple-element.218, ...), kind=kOutput, calls=%fused_computation.31.clone.1 | convolution fusion | flops 73400064 | bytes 4499972 | tf_op jit(solution)/shard_map/while/body/qhd,khd->hqk/dot_general | solution.py:84
  199.7 5.0 %fusion.63 = f32[1,256,16,128]{1,2,3,0:T(8,128)S(1)} fusion(f32[1,256,16,128]{1,3,2,0:T(8,128)S(1)} %bitcast.76), kind=kOutput, calls=%fused_computation.16.clone.1 | output fusion | flops 66584576 | bytes 4194304 | tf_op jit(solution)/shard_map/reduce-window
  207.4 4.6 %fusion.64 = bf16[256,2048]{0,1:T(8,128)(2,1)S(1)} fusion(f32[1,256,16,128]{1,3,2,0:T(8,128)} %copy.29, f32[256,2048]{0,1:T(8,128)} %get-tuple-element.181, f32[256]{0:T(256)S(1)} %bitcast.82, f32[256,16]{0,1:T(8,128)S(1)} %slice_bitcast_fusion.7, s32[256]{0:T(256)S(1)} %iota_add_fusion.4, s32[2048]{0:T(1024)S(1)} %iota_add_fusion.5), kind=kLoop, calls=%fused_computation.8.clone.1 | loop fusion | flops 12058624 | bytes 5269504 | tf_op jit(solution)/shard_map/while/body/convert_element_type | solution.py:94
  213.4 4.6 %fusion.62 = (f32[256]{0:T(256)S(1)}, f32[256,2048]{0,1:T(8,128)S(1)}, f32[256,2048]{0,1:T(8,128)}) fusion(s32[256]{0:T(256)S(1)} %iota_add_fusion.4, s32[2048]{0:T(1024)S(1)} %iota_add_fusion.5, f32[]{:T(128)} %bitcast.72, bf16[256,1,64]{0,2,1:T(8,128)(2,1)S(1)} %get-tuple-element.219, bf16[16384,1,64]{0,2,1:T(8,128)(2,1)} %get-tuple-element.218, ...), kind=kOutput, calls=%fused_computation.31.clone.1 | convolution fusion | flops 73400064 | bytes 4499972 | tf_op jit(solution)/shard_map/while/body/qhd,khd->hqk/dot_general | solution.py:84
  217.9 5.0 %fusion.63 = f32[1,256,16,128]{1,2,3,0:T(8,128)S(1)} fusion(f32[1,256,16,128]{1,3,2,0:T(8,128)S(1)} %bitcast.76), kind=kOutput, calls=%fused_computation.16.clone.1 | output fusion | flops 66584576 | bytes 4194304 | tf_op jit(solution)/shard_map/reduce-window
  225.7 4.6 %fusion.64 = bf16[256,2048]{0,1:T(8,128)(2,1)S(1)} fusion(f32[1,256,16,128]{1,3,2,0:T(8,128)} %copy.29, f32[256,2048]{0,1:T(8,128)} %get-tuple-element.181, f32[256]{0:T(256)S(1)} %bitcast.82, f32[256,16]{0,1:T(8,128)S(1)} %slice_bitcast_fusion.7, s32[256]{0:T(256)S(1)} %iota_add_fusion.4, s32[2048]{0:T(1024)S(1)} %iota_add_fusion.5), kind=kLoop, calls=%fused_computation.8.clone.1 | loop fusion | flops 12058624 | bytes 5269504 | tf_op jit(solution)/shard_map/while/body/convert_element_type | solution.py:94
  231.6 4.6 %fusion.62 = (f32[256]{0:T(256)S(1)}, f32[256,2048]{0,1:T(8,128)S(1)}, f32[256,2048]{0,1:T(8,128)}) fusion(s32[256]{0:T(256)S(1)} %iota_add_fusion.4, s32[2048]{0:T(1024)S(1)} %iota_add_fusion.5, f32[]{:T(128)} %bitcast.72, bf16[256,1,64]{0,2,1:T(8,128)(2,1)S(1)} %get-tuple-element.219, bf16[16384,1,64]{0,2,1:T(8,128)(2,1)} %get-tuple-element.218, ...), kind=kOutput, calls=%fused_computation.31.clone.1 | convolution fusion | flops 73400064 | bytes 4499972 | tf_op jit(solution)/shard_map/while/body/qhd,khd->hqk/dot_general | solution.py:84
  236.2 5.0 %fusion.63 = f32[1,256,16,128]{1,2,3,0:T(8,128)S(1)} fusion(f32[1,256,16,128]{1,3,2,0:T(8,128)S(1)} %bitcast.76), kind=kOutput, calls=%fused_computation.16.clone.1 | output fusion | flops 66584576 | bytes 4194304 | tf_op jit(solution)/shard_map/reduce-window
  243.9 4.6 %fusion.64 = bf16[256,2048]{0,1:T(8,128)(2,1)S(1)} fusion(f32[1,256,16,128]{1,3,2,0:T(8,128)} %copy.29, f32[256,2048]{0,1:T(8,128)} %get-tuple-element.181, f32[256]{0:T(256)S(1)} %bitcast.82, f32[256,16]{0,1:T(8,128)S(1)} %slice_bitcast_fusion.7, s32[256]{0:T(256)S(1)} %iota_add_fusion.4, s32[2048]{0:T(1024)S(1)} %iota_add_fusion.5), kind=kLoop, calls=%fused_computation.8.clone.1 | loop fusion | flops 12058624 | bytes 5269504 | tf_op jit(solution)/shard_map/while/body/convert_element_type | solution.py:94
  250.1 9.5 %all_to_all.26 = bf16[8,2,1024]{2,1,0:T(2,128)(2,1)S(1)} all-to-all(bf16[8,2,1024]{2,1,0:T(2,128)(2,1)S(1)} %reshape.137), channel_id=1, replica_groups=mesh['sp'=64,'tp'=8] {'tp'}, dimensions={0} | all-to-all | bytes 65536 | tf_op jit(solution)/shard_map/all_to_all | solution.py:127
  261.6 18.4 %all_to_all.27 = bf16[8,32,2048]{2,1,0:T(8,128)(2,1)S(1)} all-to-all(bf16[8,32,2048]{2,1,0:T(8,128)(2,1)S(1)} %broadcast_in_dim.16), channel_id=1, replica_groups=mesh['sp'=64,'tp'=8] {'tp'}, dimensions={0} | all-to-all | bytes 2097152 | tf_op jit(solution)/shard_map/all_to_all | solution.py:25
  280.0 3.3 %fusion.29 = bf16[256,704]{0,1:T(8,128)(2,1)S(1)} fusion(bf16[256,2048]{1,0:T(8,128)(2,1)S(1)} %bitcast.77, bf16[2048,1408]{1,0:T(8,128)(2,1)} %all-gather.6.cloned.1.call-done), kind=kOutput, calls=%fused_computation.46 | convolution fusion | flops 738377728 | bytes 4554752 | tf_op jit(solution)/shard_map/dot_general | solution.py:134
  289.5 10.7 %collective-permute-done = bf16[2,1408]{0,1:T(8,128)(2,1)S(1)} collective-permute-done((bf16[2,1408]{0,1:T(8,128)(2,1)S(1)}, bf16[2,1408]{0,1:T(8,128)(2,1)S(1)}, u32[]{:S(2)}, u32[]{:S(2)}) %collective-permute-start) | collective-permute-done | bytes 5664 | tf_op jit(solution)/shard_map/ppermute | solution.py:35
  305.3 18.5 %all_to_all.28 = bf16[8,32,2048]{2,1,0:T(8,128)(2,1)S(1)} all-to-all(bf16[8,32,2048]{2,1,0:T(8,128)(2,1)S(1)} %bitcast.79), channel_id=1, replica_groups=mesh['sp'=64,'tp'=8] {'tp'}, dimensions={0} | all-to-all | bytes 2097152 | tf_op jit(solution)/shard_map/all_to_all | solution.py:45
  (120 shorter events, 49.9 us)
Async XLA Ops:
  6.5 253.4 %copy-start = (bf16[512,2048]{1,0:T(8,128)(2,1)S(1)}, bf16[512,2048]{1,0:T(8,128)(2,1)}, u32[]{:S(2)}) copy-start(bf16[512,2048]{1,0:T(8,128)(2,1)} %param.21) | copy-start | bytes 6291460
  6.5 92.7 %all-gather.4.cloned.1.call-start = ((), (), s32[]{:S(2)}) async-start(), calls=%async_computation.3 | async-start | bytes 4259840 | tf_op jit(solution)/shard_map/all_gather | solution.py:13
  8.1 271.9 %all-gather.6.cloned.1.call-start = ((), (), s32[]{:S(2)}) async-start(), calls=%async_computation.4 | async-start | bytes 5857280 | tf_op jit(solution)/shard_map/all_gather | solution.py:13
  9.7 292.6 %all-gather.8.cloned.1.call-start = ((), (), s32[]{:S(2)}) async-start(), calls=%async_computation.5 | async-start | bytes 3194880 | tf_op jit(solution)/shard_map/all_gather | solution.py:55
  10.5 93.3 %copy-start.10 = (bf16[256,64]{0,1:T(8,128)(2,1)S(1)}, bf16[256,64]{0,1:T(8,128)(2,1)}, u32[]{:S(2)}) copy-start(bf16[256,64]{0,1:T(8,128)(2,1)} %param.16) | copy-start | bytes 98308
  249.9 10.6 %copy-start.3 = (bf16[32,2048]{1,0:T(8,128)(2,1)S(1)}, bf16[32,2048]{1,0:T(8,128)(2,1)}, u32[]{:S(2)}) copy-start(bf16[32,2048]{1,0:T(8,128)(2,1)} %param.20) | copy-start | bytes 393220
  249.9 10.6 %copy-start.6 = (f32[2048]{0:T(1024)S(1)}, f32[2048]{0:T(1024)}, u32[]{:S(2)}) copy-start(f32[2048]{0:T(1024)} %param.22) | copy-start | bytes 24580
  249.9 11.5 %copy-start.7 = (f32[2048]{0:T(1024)S(1)}, f32[2048]{0:T(1024)}, u32[]{:S(2)}) copy-start(f32[2048]{0:T(1024)} %param.23) | copy-start | bytes 24580
  260.7 0.7 copy-start.1
  280.0 3.6 %copy-start.9 = (bf16[2048,1408]{1,0:T(8,128)(2,1)S(1)}, bf16[2048,1408]{1,0:T(8,128)(2,1)}, u32[]{:S(2)}) copy-start(bf16[2048,1408]{1,0:T(8,128)(2,1)} %all-gather.6.cloned.1.call-done) | copy-start | bytes 17301508
  283.6 5.8 %copy-start.4 = (f32[3,704]{1,0:T(4,128)S(1)}, f32[3,704]{1,0:T(4,128)}, u32[]{:S(2)}) copy-start(f32[3,704]{1,0:T(4,128)} %param.27) | copy-start | bytes 25348
  283.6 5.8 %copy-start.5 = (f32[3,704]{1,0:T(4,128)S(1)}, f32[3,704]{1,0:T(4,128)}, u32[]{:S(2)}) copy-start(f32[3,704]{1,0:T(4,128)} %param.26) | copy-start | bytes 25348
  286.5 13.8 %collective-permute-start = (bf16[2,1408]{0,1:T(8,128)(2,1)S(1)}, bf16[2,1408]{0,1:T(8,128)(2,1)S(1)}, u32[]{:S(2)}, u32[]{:S(2)}) collective-permute-start(bf16[2,1408]{0,1:T(8,128)(2,1)S(1)} %pad_maximum_fusion), channel_id=1, source_target_pairs={{0,8},{8,16},{16,24},{24,32},{32,40},{40,48},{48,56},{56,64},{64,7... | collective-permute-start | bytes 16904 | tf_op jit(solution)/shard_map/ppermute | solution.py:35
  305.3 18.9 %copy-start.2 = (bf16[32,2048]{1,0:T(8,128)(2,1)S(1)}, bf16[32,2048]{1,0:T(8,128)(2,1)}, u32[]{:S(2)}) copy-start(bf16[32,2048]{1,0:T(8,128)(2,1)} %copy-done.1) | copy-start | bytes 393220
  305.3 18.8 %copy-start.8 = (f32[2048]{0:T(1024)S(1)}, f32[2048]{0:T(1024)}, u32[]{:S(2)}) copy-start(f32[2048]{0:T(1024)} %param.29) | copy-start | bytes 24580
Sparse Core Ops, SparseCore 0:
  10.3 88.8 all-gather.3
  102.2 85.3 all-gather.5
  190.6 82.1 all-gather.7
where the time goes:
time: 332 us; the launch traced here: 331 us
  waiting for transfers between devices  100 us (30%)
  other arithmetic  84.9 us (26%)
  matrix products  56 us (17%)
  blocking collectives  46.4 us (14%)
  local copies, waits for them, and re-layouts  27 us (8%)
  between operations  13.3 us (4%)
    all_gather x2, waiting for transfers between devices, side_by_side(): out = lax.all_gather(both, axis, axis=dim, tiled=True)  88.7 us
    another operation x16, other arithmetic  40.8 us
    convert_element_type x8, other arithmetic, visit(): weights = jnp.where(causal, jnp.exp(jax.nn.log_sigmoid(scores) + later +...  37.1 us
    dot_general x8, matrix products, visit(): jnp.einsum('qhd,khd->hqk', query_heads, key_block, preferred_element_type...  36.4 us
    another operation x24, local copies, waits for them, and re-layouts  21 us
    all_to_all x1, blocking collectives, sum_at_owner(): lax.all_to_all(parts, axis, split_axis=0, concat_axis=0, tiled=True)  18.5 us
    all_to_all x1, blocking collectives, from_everyone(): lax.all_to_all(jnp.broadcast_to(x[None], (length, *x.shape)), axis, 0, 0,...  18.4 us
    ppermute x1, waiting for transfers between devices, from_behind(): return lax.ppermute(x, axis, pairs)  10.7 us
  transfers between devices with their start and end apart: 4, of which 2 were waited for; matrix products, arithmetic and copies ran while one was open for 49% of the time, Pallas kernels for 0%

commit v1 on v0

v1 whole, which is shorter than its diff:
```python
import functools
import math

import jax
import jax.numpy as jnp
from jax import lax
from jax.experimental import pallas as pl
from jax.experimental.pallas import tpu as pltpu
from jax.sharding import PartitionSpec as P

HEAD_DIM = 64
KERNEL = 3
RING = 8
MESH = pl.DeviceIdType.MESH
LOG2E = 1.0 / math.log(2.0)
LANES = 128


def from_everyone(x, axis):
    length = lax.axis_size(axis)
    return lax.all_to_all(jnp.broadcast_to(x[None], (length, *x.shape)), axis, 0, 0, tiled=True)


def from_behind(x, axis, by):
    length = lax.axis_size(axis)
    pairs = [(i, i + by) for i in range(length) if 0 <= i + by < length]
    return lax.ppermute(x, axis, pairs)


def sum_at_owner(x, axis):
    length = lax.axis_size(axis)
    parts = x.reshape(length, -1, x.shape[1])
    arrived = lax.all_to_all(parts, axis, split_axis=0, concat_axis=0, tiled=True)
    return arrived.astype(jnp.float32).sum(axis=0)


def rms_scale(values_in):
    return values_in * lax.rsqrt(jnp.mean(values_in * values_in, axis=-1, keepdims=True) + 1e-06)


def wrap(v):
    return lax.rem(v + 2 * RING, RING)


class Rings:
    def __init__(self, z, y, local, buf, send, recv, base):
        self.z, self.y, self.local, self.buf = z, y, local, buf
        self.send, self.recv, self.base = send, recv, base
        rows = local.shape[0]
        self.half = (pl.ds(0, rows // 2), pl.ds(rows // 2, rows // 2))
        self.copies = {}

    def _neighbour(self, along_y, sign):
        if along_y:
            return {"sp": self.z * RING + wrap(self.y + sign)}
        return {"sp": wrap(self.z + sign) * RING + self.y}

    def _start(self, key, src, dst, along_y, sign):
        slot = self.base + len(self.copies)
        copy = pltpu.make_async_remote_copy(
            src_ref=src,
            dst_ref=dst,
            send_sem=self.send.at[slot],
            recv_sem=self.recv.at[slot],
            device_id=self._neighbour(along_y, sign),
            device_id_type=MESH,
        )
        copy.start()
        self.copies[key] = copy

    def first(self, h, sign, s):
        rows = self.half[h]
        if h == 0:
            place = self.buf.at[self.z, wrap(self.y - sign * s), rows]
        else:
            place = self.buf.at[wrap(self.z - sign * s), self.y, rows]
        src = self.local.at[rows] if s == 0 else place
        self._start((1, h, sign, s), src, place, h == 0, sign)

    def second(self, h, sign, s, c):
        rows = self.half[h]
        chunk = pl.ds(c * (RING // 2), RING // 2)
        if h == 0:
            place = self.buf.at[wrap(self.z - sign * s), chunk, rows]
        else:
            place = self.buf.at[chunk, wrap(self.y - sign * s), rows]
        self._start((2, h, sign, s, c), place, place, h == 1, sign)

    def first_step(self, s):
        for h in (0, 1):
            for sign in (1, -1):
                if s > 0 and (1, h, sign, s - 1) in self.copies:
                    self.copies[(1, h, sign, s - 1)].wait_recv()
                if s < (4 if sign == 1 else 3):
                    self.first(h, sign, s)

    def second_step(self, s, c):
        for h in (0, 1):
            for sign in (1, -1):
                if s > 0 and (2, h, sign, s - 1, c) in self.copies:
                    self.copies[(2, h, sign, s - 1, c)].wait_recv()
                if s < 3 or (s == 3 and c == (0 if sign == 1 else 1)):
                    self.second(h, sign, s, c)

    def drain(self):
        for copy in self.copies.values():
            copy.wait_send()


UNITS = 14 + 28


def tile(q_ref, kv, tri, shift2, own):
    kvb = kv[...]
    raw = lax.dot_general(
        q_ref[...], kvb, (((1,), (1,)), ((), ())), preferred_element_type=jnp.float32
    )
    t = raw * (LOG2E * HEAD_DIM**-0.5) - shift2
    soft = jnp.log(1.0 + jnp.exp2(-jnp.abs(t))) * LOG2E
    keep = jnp.maximum(t, 0.0) + soft
    sig = jnp.minimum(t, 0.0) - soft
    if own:
        row = lax.broadcasted_iota(jnp.int32, t.shape, 0)
        col = lax.broadcasted_iota(jnp.int32, t.shape, 1)
        causal = col < row
        keep = jnp.where(causal, keep, 0.0)
    sums = jnp.dot(keep.astype(jnp.bfloat16), tri[...], preferred_element_type=jnp.float32)
    span = kvb.shape[0]
    weights = jnp.exp2(sig - sums[:, :span])
    if own:
        weights = jnp.where(causal, weights, 0.0)
    return jnp.dot(
        weights.astype(jnp.bfloat16), kvb, preferred_element_type=jnp.float32
    ), sums[:, span:]


def front_kernel(
    shift_ref, q_ref, kv_ref, w_ref, att_ref, wfull, kvbuf, tri, acc, tail, send, recv, here
):
    sp = lax.axis_index("sp")
    z, y = lax.div(sp, RING), lax.rem(sp, RING)
    barrier = pltpu.get_barrier_semaphore()
    for dz, dy in ((1, 0), (-1, 0), (0, 1), (0, -1)):
        pl.semaphore_signal(
            barrier,
            inc=1,
            device_id={"sp": wrap(z + dz) * RING + wrap(y + dy)},
            device_id_type=MESH,
        )
    pl.semaphore_wait(barrier, 4)

    kv = Rings(z, y, kv_ref, kvbuf, send, recv, 0)
    w = Rings(z, y, w_ref, wfull, send, recv, UNITS)
    own_kv = pltpu.make_async_copy(kv_ref, kvbuf.at[z, y], here.at[0])
    own_w = pltpu.make_async_copy(w_ref, wfull.at[z, y], here.at[1])
    kv.first_step(0)
    w.first_step(0)
    own_kv.start()
    own_w.start()
    span = kv_ref.shape[0]
    at = lax.broadcasted_iota(jnp.int32, tri.shape, 0)
    to = lax.broadcasted_iota(jnp.int32, tri.shape, 1)
    tri[...] = jnp.where((at > to) | (to >= span), 1.0, 0.0).astype(jnp.bfloat16)
    shift2 = shift_ref[0] * LOG2E
    first_out, first_tail = tile(q_ref, kv_ref, tri, shift2, True)
    acc[...] = first_out
    tail[...] = first_tail
    for s in range(1, 4):
        kv.first_step(s)
        w.first_step(s)
    kv.first_step(4)
    own_kv.wait()
    for c in (0, 1):
        kv.second_step(0, c)
    w.first_step(4)
    own_w.wait()
    for s in range(1, 4):
        for c in (0, 1):
            kv.second_step(s, c)
    for c in (0, 1):
        w.second_step(0, c)
    for c in (0, 1):
        kv.second_step(4, c)

    def visit(turn, carry):
        block = sp - turn
        out, total = tile(
            q_ref, kvbuf.at[lax.div(block, RING), lax.rem(block, RING)], tri, shift2, False
        )
        acc[...] += jnp.exp2(-tail[...]) * out
        tail[...] += total
        return carry

    def visits(low, high):
        lax.fori_loop(low, jnp.minimum(high, sp + 1), visit, 0)

    visits(1, 33)
    w.second_step(1, 0)
    visits(33, 65)
    w.second_step(1, 1)
    att_ref[...] = acc[:, HEAD_DIM:].astype(jnp.bfloat16)
    for s in (2, 3, 4):
        for c in (0, 1):
            w.second_step(s, c)
    kv.drain()
    w.drain()


def front(queries, keys, values, score_shift, packed):
    rows = queries.shape[0]
    wide = packed.shape[1]
    vmem = pl.BlockSpec(memory_space=pltpu.VMEM)
    return pl.pallas_call(
        front_kernel,
        out_shape=(
            jax.ShapeDtypeStruct((rows, HEAD_DIM), jnp.bfloat16),
            jax.ShapeDtypeStruct((RING, RING, packed.shape[0], wide), jnp.bfloat16),
        ),
        in_specs=[pl.BlockSpec(memory_space=pltpu.SMEM), vmem, vmem, vmem],
        out_specs=(vmem, vmem),
        scratch_shapes=[
            pltpu.VMEM((RING, RING, rows, LANES), jnp.bfloat16),
            pltpu.VMEM((rows, rows + LANES), jnp.bfloat16),
            pltpu.VMEM((rows, LANES), jnp.float32),
            pltpu.VMEM((rows, LANES), jnp.float32),
            pltpu.SemaphoreType.DMA((2 * UNITS,)),
            pltpu.SemaphoreType.DMA((2 * UNITS,)),
            pltpu.SemaphoreType.DMA((2,)),
        ],
        compiler_params=pltpu.CompilerParams(
            collective_id=0, has_side_effects=True, vmem_limit_bytes=48 * 1024 * 1024
        ),
        name="front",
    )(
        score_shift,
        jnp.pad(queries, ((0, 0), (0, LANES - HEAD_DIM))),
        jnp.concatenate([keys, values], axis=1),
        packed,
    )


def local(
    queries,
    keys,
    values,
    score_shift,
    resid,
    w_out,
    gain_mix,
    gain_pre,
    w_gate,
    w_up,
    conv_gate,
    conv_up,
    w_down,
    gain_post,
):
    units = w_gate.shape[1]
    pad = -(3 * units) % LANES
    packed = jnp.concatenate(
        [w_gate, w_up, w_down.T, jnp.zeros((w_gate.shape[0], pad), jnp.bfloat16)], axis=1
    )
    attended, whole = front(queries, keys, values, score_shift, packed)
    whole = whole.reshape(-1, packed.shape[1])
    head_rows = lax.all_to_all(attended, "tp", split_axis=0, concat_axis=1, tiled=True)
    mixed = jnp.dot(head_rows, w_out, preferred_element_type=jnp.float32).astype(jnp.bfloat16)
    middle = (resid.astype(jnp.float32) + gain_mix * rms_scale(mixed.astype(jnp.float32))).astype(
        jnp.bfloat16
    )
    normed = (gain_pre * rms_scale(middle.astype(jnp.float32))).astype(jnp.bfloat16)
    piece = from_everyone(normed, "tp").reshape(-1, normed.shape[1])
    projected = jnp.dot(
        piece, whole[:, : 2 * units], preferred_element_type=jnp.float32
    ).astype(jnp.bfloat16)
    tok_rows = projected.shape[0]
    edge = from_behind(projected[tok_rows - (KERNEL - 1) :], "sp", 1)
    extended = jnp.concatenate([edge, projected], axis=0).astype(jnp.float32)
    taps = jnp.concatenate([conv_gate, conv_up], axis=1)
    convolved = taps[0] * extended[0:tok_rows]
    for tap in range(1, KERNEL):
        convolved = convolved + taps[tap] * extended[tap : tap + tok_rows]
    hidden = (jax.nn.silu(convolved[:, :units]) * convolved[:, units:]).astype(jnp.bfloat16)
    partial = lax.dot_general(
        hidden,
        whole[:, 2 * units : 3 * units],
        (((1,), (1,)), ((), ())),
        preferred_element_type=jnp.float32,
    ).astype(jnp.bfloat16)
    ffn_out = sum_at_owner(partial, "tp").astype(jnp.bfloat16)
    return (middle.astype(jnp.float32) + gain_post * rms_scale(ffn_out.astype(jnp.float32))).astype(
        jnp.bfloat16
    )


def solution(mesh):
    in_specs = (
        P("sp", "tp"),
        P("sp", "tp"),
        P("sp", "tp"),
        P("tp"),
        P(("sp", "tp"), None),
        P(),
        P(),
        P(),
        P("sp", "tp"),
        P("sp", "tp"),
        P(None, "tp"),
        P(None, "tp"),
        P("tp", "sp"),
        P(),
    )
    out_specs = P(("sp", "tp"), None)
    return jax.shard_map(local, mesh=mesh, in_specs=in_specs, out_specs=out_specs, check_vma=False)
```

time: 332 us -> 179 us (0.54)
  the two profiles are of different devices: /device:TPU:448 before, /device:TPU:1 now
where the time goes in v1:
time: 179 us; the launch traced here: 177 us
  Pallas kernels  100 us (56%)
  blocking collectives  57.9 us (32%)
  matrix products  7.95 us (4%)
  local copies, waits for them, and re-layouts  4.13 us (2%)
  starting transfers between devices  3.13 us (2%)
  other arithmetic  2.19 us (1%)
    pallas_call x1, Pallas kernels, front(): pl.pallas_call(front_kernel, out_shape=(jax.ShapeDtypeStruct((rows, HEAD_...  100 us
    all_to_all x1, blocking collectives, local(): lax.all_to_all(attended, 'tp', split_axis=0, concat_axis=1, tiled=True)  20.6 us
    all_to_all x1, blocking collectives, sum_at_owner(): lax.all_to_all(parts, axis, split_axis=0, concat_axis=0, tiled=True)  19.2 us
    all_to_all x1, blocking collectives, from_everyone(): lax.all_to_all(jnp.broadcast_to(x[None], (length, *x.shape)), axis, 0, 0,...  18.1 us
    dot_general x1, matrix products, local(): jnp.dot(piece, whole[:, :2 * units], preferred_element_type=jnp.float32)  4.45 us
  transfers between devices with their start and end apart: 1, of which 1 were waited for; matrix products, arithmetic and copies ran while one was open for 0% of the time, Pallas kernels for 0%

profile of v1, /device:TPU:1, one launch (start us, length us, event | category | flops | bytes accessed | tf_op | source)
XLA Modules:
  0.0 176.9 jit_solution(17371407322952621401)
XLA Ops:
  0.8 0.9 copy.22
  1.7 0.9 copy.23
  2.6 0.9 copy.24
  3.5 0.1 pad_maximum_fusion.kv_ref
  3.6 1.0 concatenate.13.w_ref
  4.5 100.0 %front.1 = (bf16[256,64]{1,0:T(8,128)(2,1)S(1)}, bf16[8,8,32,2176]{3,2,1,0:T(8,128)(2,1)}) custom-call(f32[1]{0:T(128)S(6)} %copy.26.shift_ref, bf16[256,128]{1,0:T(8,128)(2,1)S(1)} %pad.4.q_ref, bf16[256,128]{1,0:T(8,128)(2,1)S(1)} %pad_maximum_fusion.kv_ref, bf16[32,2176]{1,0:T(8,128)(2,1)S(1)} %concatenate.13.w_ref), custom_call_target="tpu_custom_call" | custom-call | tf_op jit(solution)/shard_map/front/pallas_call | solution.py:213
  104.6 0.0 copy-start.1
  104.6 0.0 copy-start.4
  104.6 0.1 reshape.46
  104.7 20.6 %all_to_all.29 = bf16[8,2,1024]{2,1,0:T(2,128)(2,1)S(1)} all-to-all(bf16[8,2,1024]{2,1,0:T(2,128)(2,1)S(1)} %reshape.46), channel_id=1, replica_groups=mesh['sp'=64,'tp'=8] {'tp'}, dimensions={0} | all-to-all | bytes 65536 | tf_op jit(solution)/shard_map/all_to_all | solution.py:265
  125.3 0.1 reshape.47
  125.4 0.1 all_to_all.23
  125.5 0.0 copy-start.5
  125.5 0.6 multiply_reduce_fusion
  126.2 0.2 fusion.18
  126.4 0.1 fusion.20
  126.5 0.1 broadcast_in_dim.5
  126.6 18.1 %all_to_all.30 = bf16[8,32,2048]{2,1,0:T(8,128)(2,1)S(1)} all-to-all(bf16[8,32,2048]{2,1,0:T(8,128)(2,1)S(1)} %broadcast_in_dim.5), channel_id=1, replica_groups=mesh['sp'=64,'tp'=8] {'tp'}, dimensions={0} | all-to-all | bytes 2097152 | tf_op jit(solution)/shard_map/all_to_all | solution.py:21
  144.7 4.4 %fusion.4 = bf16[256,1408]{1,0:T(8,128)(2,1)S(1)} fusion(bf16[256,2048]{1,0:T(8,128)(2,1)S(1)} %bitcast.10, bf16[2048,2176]{1,0:T(8,128)(2,1)} %bitcast.14), kind=kOutput, calls=%fused_computation.4 | convolution fusion | flops 1476755456 | bytes 7536640 | tf_op jit(solution)/shard_map/dot_general | solution.py:272
  149.2 3.1 %collective-permute-start = (bf16[2,1408]{1,0:T(2,128)(2,1)S(1)}, bf16[2,1408]{1,0:T(2,128)(2,1)S(1)}, u32[]{:S(2)}, u32[]{:S(2)}) collective-permute-start(bf16[2,1408]{1,0:T(2,128)(2,1)S(1)} %slice.45), channel_id=1, source_target_pairs={{0,8},{8,16},{16,24},{24,32},{32,40},{40,48},{48,56},{56,64},{64,7... | collective-permute-start | bytes 16904 | tf_op jit(solution)/shard_map/ppermute | solution.py:27
  152.3 0.0 copy-done.2
  152.3 0.0 copy-done.3
  152.3 0.1 maximum_reduce_fusion.1
  152.4 0.6 collective-permute-done
  153.1 0.1 maximum_convert_fusion
  153.2 0.4 fusion.11
  153.7 2.9 %fusion.7 = bf16[256,2048]{1,0:T(8,128)(2,1)S(1)} fusion(bf16[2048,2176]{1,0:T(8,128)(2,1)} %bitcast.15, f32[256,1408]{1,0:T(8,128)S(1)} %fusion.11), kind=kOutput, calls=%fused_computation.5 | convolution fusion | flops 739803136 | bytes 5767168 | tf_op jit(solution)/shard_map/dot_general | solution.py:283
  156.6 0.0 copy-start.6
  156.6 19.2 %all_to_all.31 = bf16[8,32,2048]{2,1,0:T(8,128)(2,1)S(1)} all-to-all(bf16[8,32,2048]{2,1,0:T(8,128)(2,1)S(1)} %bitcast.11), channel_id=1, replica_groups=mesh['sp'=64,'tp'=8] {'tp'}, dimensions={0} | all-to-all | bytes 2097152 | tf_op jit(solution)/shard_map/all_to_all | solution.py:33
  175.9 0.1 reduce_sum.41
  176.0 0.1 fusion.16
  176.2 0.8 fusion.21
  (15 shorter events, 0.1 us)
Async XLA Ops:
  0.0 125.5 %copy-start = (bf16[512,2048]{1,0:T(8,128)(2,1)S(1)}, bf16[512,2048]{1,0:T(8,128)(2,1)}, u32[]{:S(2)}) copy-start(bf16[512,2048]{1,0:T(8,128)(2,1)} %param.19) | copy-start | bytes 6291460
  104.6 21.6 %copy-start.1 = (bf16[32,2048]{1,0:T(8,128)(2,1)S(1)}, bf16[32,2048]{1,0:T(8,128)(2,1)}, u32[]{:S(2)}) copy-start(bf16[32,2048]{1,0:T(8,128)(2,1)} %param.18) | copy-start | bytes 393220
  104.6 21.6 %copy-start.4 = (f32[2048]{0:T(1024)S(1)}, f32[2048]{0:T(1024)}, u32[]{:S(2)}) copy-start(f32[2048]{0:T(1024)} %param.20) | copy-start | bytes 24580
  125.5 0.9 copy-start.5
  144.7 7.6 %copy-start.2 = (f32[3,704]{1,0:T(4,128)S(1)}, f32[3,704]{1,0:T(4,128)}, u32[]{:S(2)}) copy-start(f32[3,704]{1,0:T(4,128)} %param.25) | copy-start | bytes 25348
  144.7 7.6 %copy-start.3 = (f32[3,704]{1,0:T(4,128)S(1)}, f32[3,704]{1,0:T(4,128)}, u32[]{:S(2)}) copy-start(f32[3,704]{1,0:T(4,128)} %param.24) | copy-start | bytes 25348
  149.2 3.9 %collective-permute-start = (bf16[2,1408]{1,0:T(2,128)(2,1)S(1)}, bf16[2,1408]{1,0:T(2,128)(2,1)S(1)}, u32[]{:S(2)}, u32[]{:S(2)}) collective-permute-start(bf16[2,1408]{1,0:T(2,128)(2,1)S(1)} %slice.45), channel_id=1, source_target_pairs={{0,8},{8,16},{16,24},{24,32},{32,40},{40,48},{48,56},{56,64},{64,7... | collective-permute-start | bytes 16904 | tf_op jit(solution)/shard_map/ppermute | solution.py:27
  156.6 19.6 %copy-start.6 = (f32[2048]{0:T(1024)S(1)}, f32[2048]{0:T(1024)}, u32[]{:S(2)}) copy-start(f32[2048]{0:T(1024)} %param.27) | copy-start | bytes 24580

commit v2 on v0

v2 whole, which is shorter than its diff:
```python
import math

import jax
import jax.numpy as jnp
from jax import lax
from jax.experimental import pallas as pl
from jax.experimental.pallas import tpu as pltpu
from jax.sharding import PartitionSpec as P

HEAD_DIM = 64
KERNEL = 3
RING = 8
CHIPS = 4
GROUP = 8
MESH = pl.DeviceIdType.MESH
LOG2E = 1.0 / math.log(2.0)
LANES = 128
HALO = 16
UNROLL = 4
TRANSFERS = 256
LOADS = 8


def wrap(v, n):
    return lax.rem(v + 2 * n, n)


class Post:
    def __init__(self, send, recv):
        self.send, self.recv, self.copies = send, recv, []

    def start(self, src, dst, device):
        slot = len(self.copies)
        copy = pltpu.make_async_remote_copy(
            src_ref=src,
            dst_ref=dst,
            send_sem=self.send.at[slot],
            recv_sem=self.recv.at[slot],
            device_id=device,
            device_id_type=MESH,
        )
        copy.start()
        self.copies.append(copy)
        return copy

    def drain(self):
        for copy in self.copies:
            copy.wait_send()


class Rings:
    def __init__(self, post, z, y, buf):
        self.post, self.z, self.y, self.buf = post, z, y, buf
        rows = buf.shape[2]
        self.half = (pl.ds(0, rows // 2), pl.ds(rows // 2, rows // 2))
        self.copies = {}

    def _neighbour(self, along_y, sign):
        if along_y:
            return {"sp": self.z * RING + wrap(self.y + sign, RING)}
        return {"sp": wrap(self.z + sign, RING) * RING + self.y}

    def first(self, h, sign, s):
        rows = self.half[h]
        if h == 0:
            place = self.buf.at[self.z, wrap(self.y - sign * s, RING), rows]
        else:
            place = self.buf.at[wrap(self.z - sign * s, RING), self.y, rows]
        self.copies[(1, h, sign, s)] = self.post.start(place, place, self._neighbour(h == 0, sign))

    def second(self, h, sign, s, c):
        rows = self.half[h]
        chunk = pl.ds(c * (RING // 2), RING // 2)
        if h == 0:
            place = self.buf.at[wrap(self.z - sign * s, RING), chunk, rows]
        else:
            place = self.buf.at[chunk, wrap(self.y - sign * s, RING), rows]
        self.copies[(2, h, sign, s, c)] = self.post.start(
            place, place, self._neighbour(h == 1, sign)
        )

    def first_step(self, s):
        for h in (0, 1):
            for sign in (1, -1):
                if (1, h, sign, s - 1) in self.copies:
                    self.copies[(1, h, sign, s - 1)].wait_recv()
                if s < (4 if sign == 1 else 3):
                    self.first(h, sign, s)

    def second_step(self, s, c):
        for h in (0, 1):
            for sign in (1, -1):
                if (2, h, sign, s - 1, c) in self.copies:
                    self.copies[(2, h, sign, s - 1, c)].wait_recv()
                if s < 3 or (s == 3 and c == (0 if sign == 1 else 1)):
                    self.second(h, sign, s, c)


def tile(query, pair, tri, shift2, own):
    raw = jnp.dot(query, pair, preferred_element_type=jnp.float32)
    t = raw * (LOG2E * HEAD_DIM**-0.5) - shift2
    spent = jnp.maximum(t, jnp.log(1.0 + jnp.exp2(jnp.minimum(t, 126.0))) * LOG2E)
    taken = t - spent
    if own:
        row = lax.broadcasted_iota(jnp.int32, t.shape, 0)
        col = lax.broadcasted_iota(jnp.int32, t.shape, 1)
        causal = col < row
        spent = jnp.where(causal, spent, 0.0)
    later = jnp.dot(spent.astype(jnp.bfloat16), tri, preferred_element_type=jnp.float32)
    weights = jnp.exp2(taken - later)
    if own:
        weights = jnp.where(causal, weights, 0.0)
    total = jnp.broadcast_to(later[:, :1] + spent[:, :1], (t.shape[0], LANES))
    out = lax.dot_general(
        weights.astype(jnp.bfloat16),
        pair,
        (((1,), (1,)), ((), ())),
        preferred_element_type=jnp.float32,
    )
    return out, total


def rms_scale(v):
    return v * lax.rsqrt(jnp.mean(v * v, axis=-1, keepdims=True) + 1e-06)


def rounded(v):
    return v.astype(jnp.bfloat16).astype(jnp.float32)


def layer_kernel(
    shift_ref,
    gain_mix,
    gain_pre,
    gain_post,
    conv_gate,
    conv_up,
    q_hbm,
    k_hbm,
    v_hbm,
    gate_hbm,
    up_hbm,
    down_hbm,
    resid_hbm,
    wout_hbm,
    result,
    qt,
    query,
    pairs,
    gate,
    up,
    down,
    whole,
    resid,
    wout,
    tri,
    acc,
    tail,
    attended,
    arrived,
    piece,
    middle,
    edge_out,
    edge_in,
    extended,
    hidden,
    partial,
    partner_partial,
    summed,
    landed,
    passed,
    send,
    recv,
    load,
    edge_sem,
):
    sp, tp = lax.axis_index("sp"), lax.axis_index("tp")
    z, y = lax.div(sp, RING), lax.rem(sp, RING)
    x, core = lax.div(tp, 2), lax.rem(tp, 2)
    shards = RING * RING
    span = query.shape[0]
    own_rows = result.shape[0]
    width = gate.shape[1]
    mains = width // LANES
    rest = width - mains * LANES

    loads = [
        pltpu.make_async_copy(a, b, load.at[i])
        for i, (a, b) in enumerate(
            (
                (k_hbm, pairs.at[z, y, pl.ds(0, HEAD_DIM)]),
                (v_hbm, pairs.at[z, y, pl.ds(HEAD_DIM, HEAD_DIM)]),
                (gate_hbm, gate),
                (up_hbm, up),
                (down_hbm, down),
                (q_hbm, qt),
                (resid_hbm, resid),
                (wout_hbm, wout),
            )
        )
    ]
    for copy in loads:
        copy.start()
    barrier = pltpu.get_barrier_semaphore()
    greeted = [
        {"sp": wrap(z + dz, RING) * RING + wrap(y + dy, RING)}
        for dz, dy in ((1, 0), (-1, 0), (0, 1), (0, -1))
    ]
    greeted += [{"sp": wrap(sp + 1, shards)}, {"sp": wrap(sp - 1, shards)}]
    greeted += [{"tp": wrap(tp + k, GROUP)} for k in range(1, GROUP)]
    for device in greeted:
        pl.semaphore_signal(barrier, inc=1, device_id=device, device_id_type=MESH)
    for copy in loads[2:5]:
        copy.wait()
    for j in range(mains):
        here = slice(j * LANES, (j + 1) * LANES)
        whole[z, y, :, 2 * j * LANES : (2 * j + 1) * LANES] = gate[:, here]
        whole[z, y, :, (2 * j + 1) * LANES : (2 * j + 2) * LANES] = up[:, here]
    base = 2 * mains * LANES
    whole[z, y, :, base : base + LANES] = jnp.concatenate(
        [gate[:, mains * LANES :], up[:, mains * LANES :]], axis=1
    )
    down_at = base + LANES
    whole[z, y, :, down_at : down_at + mains * LANES] = down[:, : mains * LANES]
    whole[z, y, :, down_at + mains * LANES :] = jnp.concatenate(
        [down[:, mains * LANES :], jnp.zeros((down.shape[0], LANES - rest), jnp.bfloat16)], axis=1
    )
    for copy in loads[:2]:
        copy.wait()
    pl.semaphore_wait(barrier, len(greeted))

    post = Post(send, recv)
    kv = Rings(post, z, y, pairs)
    w = Rings(post, z, y, whole)
    kv.first_step(0)
    w.first_step(0)

    at = lax.broadcasted_iota(jnp.int32, tri.shape, 0)
    to = lax.broadcasted_iota(jnp.int32, tri.shape, 1)
    tri[...] = jnp.where(at > to, 1.0, 0.0).astype(jnp.bfloat16)
    loads[5].wait()
    padded = jnp.concatenate(
        [qt[...].astype(jnp.float32), jnp.zeros(qt.shape, jnp.float32)], axis=0
    )
    query[...] = padded.T.astype(jnp.bfloat16)
    shift2 = shift_ref[0] * LOG2E
    kv.first_step(1)
    w.first_step(1)
    first_out, first_tail = tile(query[...], pairs[z, y], tri[...], shift2, True)
    acc[...] = first_out
    tail[...] = first_tail
    for s in (2, 3):
        kv.first_step(s)
        w.first_step(s)
    kv.first_step(4)
    for c in (0, 1):
        kv.second_step(0, c)
    w.first_step(4)
    for s in (1, 2, 3):
        for c in (0, 1):
            kv.second_step(s, c)
    for c in (0, 1):
        w.second_step(0, c)
    for c in (0, 1):
        kv.second_step(4, c)

    def visit(first, count):
        found = []
        for k in range(count):
            block = sp - first - k
            pair = pairs[lax.div(block, RING), lax.rem(block, RING)]
            found.append(tile(query[...], pair, tri[...], shift2, False))
        total, spent = acc[...], tail[...]
        for out, more in found:
            total = total + jnp.exp2(-spent) * out
            spent = spent + more
        acc[...] = total
        tail[...] = spent

    odd = lax.rem(sp, UNROLL)
    many = lax.div(sp, UNROLL)

    def one(turn, carry):
        visit(turn + 1, 1)
        return carry

    def several(turn, carry):
        visit(1 + odd + turn * UNROLL, UNROLL)
        return carry

    lax.fori_loop(0, odd, one, 0)
    lax.fori_loop(0, jnp.minimum(many, 6), several, 0)
    w.second_step(1, 0)
    lax.fori_loop(6, jnp.minimum(many, 11), several, 0)
    w.second_step(1, 1)
    lax.fori_loop(11, many, several, 0)

    lane = lax.broadcasted_iota(jnp.int32, acc.shape, 1)
    mine = lax.div(lane, HEAD_DIM) == core
    turned = jnp.where(core == 0, pltpu.roll(acc[...], HEAD_DIM, axis=1), acc[...])
    attended[...] = jnp.where(mine, turned, 0.0).astype(jnp.bfloat16)
    exchange = []
    for k in range(1, GROUP):
        peer = wrap(tp + k, GROUP)
        rows = pl.ds(pl.multiple_of(peer * own_rows, own_rows), own_rows)
        exchange.append(post.start(attended.at[rows], arrived.at[tp], {"tp": peer}))
    arrived[tp] = attended[pl.ds(pl.multiple_of(tp * own_rows, own_rows), own_rows), :]
    w.second_step(2, 0)
    loads[6].wait()
    loads[7].wait()
    for copy in exchange:
        copy.wait_recv()
    heads = jnp.concatenate([arrived[2 * i] + arrived[2 * i + 1] for i in range(CHIPS)], axis=1)
    mixed = rounded(jnp.dot(heads, wout[...], preferred_element_type=jnp.float32))
    mid = rounded(resid[...].astype(jnp.float32) + gain_mix[...] * rms_scale(mixed))
    middle[...] = mid
    normed = rounded(gain_pre[...] * rms_scale(mid))

    right, left = wrap(x + 1, CHIPS), wrap(x - 1, CHIPS)

    def rows_of(chip, c, half=None):
        start = HALO + (2 * chip + c) * own_rows
        if half is None:
            return piece.at[pl.ds(pl.multiple_of(start, HALO), own_rows)]
        start = start + half * (own_rows // 2)
        return piece.at[pl.ds(pl.multiple_of(start, HALO), own_rows // 2)]

    def to_chip(chip):
        return {"tp": 2 * chip + core}

    partner = {"tp": 2 * x + 1 - core}

    def move(ref, device):
        return post.start(ref, ref, device)

    piece[pl.ds(pl.multiple_of(HALO + tp * own_rows, HALO), own_rows), :] = normed.astype(
        jnp.bfloat16
    )
    edge_out[...] = normed[own_rows - (KERNEL - 1) :, :]
    plus = [move(rows_of(x, core, 0), to_chip(right))]
    minus = [move(rows_of(x, core, 1), to_chip(left))]
    plus.append(move(rows_of(x, core, 1), to_chip(right)))
    minus.append(move(rows_of(x, core, 0), to_chip(left)))
    across = [move(rows_of(x, core), partner)]

    def edge_copy(src, device, slot):
        return pltpu.make_async_remote_copy(
            src_ref=src,
            dst_ref=edge_in,
            send_sem=edge_sem.at[slot],
            recv_sem=edge_sem.at[GROUP],
            device_id=device,
            device_id_type=MESH,
        )

    last = tp == GROUP - 1
    ahead = edge_copy(edge_out, {"sp": wrap(sp + 1, shards)}, 0)

    @pl.when(last & (sp < shards - 1))
    def _():
        ahead.start()

    w.second_step(2, 1)
    plus[0].wait_recv()
    plus.append(move(rows_of(left, core, 0), to_chip(right)))
    across.append(move(rows_of(left, core, 0), partner))
    minus[0].wait_recv()
    minus.append(move(rows_of(right, core, 1), to_chip(left)))
    across.append(move(rows_of(right, core, 1), partner))
    plus[1].wait_recv()
    across.append(move(rows_of(left, core, 1), partner))
    minus[1].wait_recv()
    across.append(move(rows_of(right, core, 0), partner))
    far = wrap(x + 2, CHIPS)
    plus[2].wait_recv()
    across.append(move(rows_of(far, core, 0), partner))
    minus[2].wait_recv()
    across.append(move(rows_of(far, core, 1), partner))
    w.second_step(3, 0)

    spread = [edge_copy(edge_in, {"tp": wrap(tp + k, GROUP)}, k) for k in range(1, GROUP)]

    @pl.when(sp > 0)
    def _():
        spread[0].wait_recv()

        @pl.when(last)
        def _():
            for copy in spread:
                copy.start()

    behind = edge_in[...]
    place = lax.broadcasted_iota(jnp.int32, (HALO, piece.shape[1]), 0)
    front = jnp.where(sp > 0, 1, 0)
    filled = jnp.where(
        (place == HALO - 1) & (front == 1),
        behind[1:2, :],
        jnp.where((place == HALO - 2) & (front == 1), behind[0:1, :], 0.0),
    )
    piece[0:HALO, :] = filled.astype(jnp.bfloat16)
    for copy in across:
        copy.wait_recv()
    w.second_step(3, 1)
    w.second_step(4, 0)
    w.second_step(4, 1)

    depth = piece.shape[1]

    def convolve(low, high, taps):
        rows = partial.shape[0] * own_rows
        found = 0.0
        for tap in range(KERNEL):
            found = found + taps[tap : tap + 1, :] * extended[
                pl.ds(HALO - KERNEL + 1 + tap, rows), low:high
            ]
        return found

    def silu(v):
        return v / (1.0 + jnp.exp(-v))

    for j in range(mains):
        cols = slice(2 * j * LANES, (2 * j + 2) * LANES)
        rhs = whole[:, :, :, cols].reshape(depth, 2 * LANES)
        extended[...] = rounded(jnp.dot(piece[...], rhs, preferred_element_type=jnp.float32))
        here = slice(j * LANES, (j + 1) * LANES)
        g = convolve(0, LANES, conv_gate[:, here])
        u = convolve(LANES, 2 * LANES, conv_up[:, here])
        hidden[:, here] = (silu(g) * u).astype(jnp.bfloat16)
    rhs = whole[:, :, :, base : base + LANES].reshape(depth, LANES)
    extended[:, :LANES] = rounded(jnp.dot(piece[...], rhs, preferred_element_type=jnp.float32))
    taps = jnp.concatenate([conv_gate[:, mains * LANES :], conv_up[:, mains * LANES :]], axis=1)
    both = convolve(0, LANES, taps)
    product = silu(both) * pltpu.roll(both, LANES - rest, axis=1)
    inside = lax.broadcasted_iota(jnp.int32, product.shape, 1) < rest
    hidden[:, mains * LANES :] = jnp.where(inside, product, 0.0).astype(jnp.bfloat16)

    for j in range(RING):
        rhs = whole[j, :, :, down_at:].reshape(depth // RING, hidden.shape[1])
        found = lax.dot_general(
            hidden[...], rhs, (((1,), (1,)), ((), ())), preferred_element_type=jnp.float32
        )
        partial[:, :, j * (depth // RING) : (j + 1) * (depth // RING)] = found.astype(
            jnp.bfloat16
        ).reshape(partial.shape[0], own_rows, depth // RING)

    swaps = [
        post.start(partial.at[2 * chip + 1 - core], partner_partial.at[chip], partner)
        for chip in range(CHIPS)
    ]
    halves = (pl.ds(0, own_rows // 2), pl.ds(own_rows // 2, own_rows // 2))
    for copy in swaps:
        copy.wait_recv()
    for chip in range(CHIPS):
        summed[chip] = (
            partial[2 * chip + core].astype(jnp.float32)
            + partner_partial[chip].astype(jnp.float32)
        ).astype(jnp.bfloat16)

    def give(src, slot, chip):
        return post.start(src, landed.at[slot], to_chip(chip))

    got = [
        give(summed.at[far, halves[0]], 0, right),
        give(summed.at[far, halves[1]], 1, left),
        give(summed.at[right, halves[1]], 2, right),
        give(summed.at[left, halves[0]], 3, left),
    ]
    got[0].wait_recv()
    passed[0] = (
        summed[right, halves[0], :].astype(jnp.float32) + landed[0].astype(jnp.float32)
    ).astype(jnp.bfloat16)
    got.append(give(passed.at[0], 4, right))
    got[1].wait_recv()
    passed[1] = (
        summed[left, halves[1], :].astype(jnp.float32) + landed[1].astype(jnp.float32)
    ).astype(jnp.bfloat16)
    got.append(give(passed.at[1], 5, left))
    for copy in got[2:]:
        copy.wait_recv()
    for h, (near, through) in enumerate(((3, 4), (2, 5))):
        ffn = rounded(
            summed[x, halves[h], :].astype(jnp.float32)
            + landed[near].astype(jnp.float32)
            + landed[through].astype(jnp.float32)
        )
        result[halves[h], :] = (
            middle[halves[h], :] + gain_post[...] * rms_scale(ffn)
        ).astype(jnp.bfloat16)

    post.drain()

    @pl.when(last & (sp < shards - 1))
    def _():
        ahead.wait_send()

    @pl.when(last & (sp > 0))
    def _():
        for copy in spread:
            copy.wait_send()


def local(
    queries,
    keys,
    values,
    score_shift,
    resid,
    w_out,
    gain_mix,
    gain_pre,
    w_gate,
    w_up,
    conv_gate,
    conv_up,
    w_down,
    gain_post,
):
    span = queries.shape[0]
    own_rows, depth = resid.shape
    width = w_gate.shape[1]
    mains = width // LANES
    slab = w_gate.shape[0]
    columns = 2 * mains * LANES + LANES + (mains + 1) * LANES
    vmem = pl.BlockSpec(memory_space=pltpu.VMEM)
    anywhere = pl.BlockSpec(memory_space=pl.ANY)
    bf16, f32 = jnp.bfloat16, jnp.float32
    return pl.pallas_call(
        layer_kernel,
        out_shape=jax.ShapeDtypeStruct((own_rows, depth), bf16),
        in_specs=[pl.BlockSpec(memory_space=pltpu.SMEM)] + [vmem] * 5 + [anywhere] * 8,
        out_specs=vmem,
        scratch_shapes=[
            pltpu.VMEM((HEAD_DIM, span), bf16),
            pltpu.VMEM((span, LANES), bf16),
            pltpu.VMEM((RING, RING, 2 * HEAD_DIM, span), bf16),
            pltpu.VMEM((slab, width), bf16),
            pltpu.VMEM((slab, width), bf16),
            pltpu.VMEM((slab, width), bf16),
            pltpu.VMEM((RING, RING, slab, columns), bf16),
            pltpu.VMEM((own_rows, depth), bf16),
            pltpu.VMEM(w_out.shape, bf16),
            pltpu.VMEM((span, span), bf16),
            pltpu.VMEM((span, LANES), f32),
            pltpu.VMEM((span, LANES), f32),
            pltpu.VMEM((span, LANES), bf16),
            pltpu.VMEM((GROUP, own_rows, LANES), bf16),
            pltpu.VMEM((HALO + span, depth), bf16),
            pltpu.VMEM((own_rows, depth), f32),
            pltpu.VMEM((KERNEL - 1, depth), f32),
            pltpu.VMEM((KERNEL - 1, depth), f32),
            pltpu.VMEM((HALO + span, 2 * LANES), f32),
            pltpu.VMEM((span, (mains + 1) * LANES), bf16),
            pltpu.VMEM((GROUP, own_rows, depth), bf16),
            pltpu.VMEM((CHIPS, own_rows, depth), bf16),
            pltpu.VMEM((CHIPS, own_rows, depth), bf16),
            pltpu.VMEM((6, own_rows // 2, depth), bf16),
            pltpu.VMEM((2, own_rows // 2, depth), bf16),
            pltpu.SemaphoreType.DMA((TRANSFERS,)),
            pltpu.SemaphoreType.DMA((TRANSFERS,)),
            pltpu.SemaphoreType.DMA((LOADS,)),
            pltpu.SemaphoreType.DMA((GROUP + 1,)),
        ],
        compiler_params=pltpu.CompilerParams(
            collective_id=0, has_side_effects=True, vmem_limit_bytes=52 * 1024 * 1024
        ),
        name="layer",
    )(
        score_shift,
        gain_mix[None],
        gain_pre[None],
        gain_post[None],
        conv_gate,
        conv_up,
        queries.T,
        keys.T,
        values.T,
        w_gate,
        w_up,
        w_down.T,
        resid,
        w_out,
    )


def solution(mesh):
    in_specs = (
        P("sp", "tp"),
        P("sp", "tp"),
        P("sp", "tp"),
        P("tp"),
        P(("sp", "tp"), None),
        P(),
        P(),
        P(),
        P("sp", "tp"),
        P("sp", "tp"),
        P(None, "tp"),
        P(None, "tp"),
        P("tp", "sp"),
        P(),
    )
    out_specs = P(("sp", "tp"), None)
    return jax.shard_map(local, mesh=mesh, in_specs=in_specs, out_specs=out_specs, check_vma=False)
```

time: 332 us -> 120 us (0.36)
  the two profiles are of different devices: /device:TPU:448 before, /device:TPU:1 now
where the time goes in v2:
time: 120 us; the launch traced here: 119 us
  Pallas kernels  109 us (91%)
  local copies, waits for them, and re-layouts  9.72 us (8%)
    pallas_call x1, Pallas kernels, local(): pl.pallas_call(layer_kernel, out_shape=jax.ShapeDtypeStruct((own_rows, de...  109 us
    unnamed x25, local copies, waits for them, and re-layouts  9.72 us

profile of v2, /device:TPU:1, one launch (start us, length us, event | category | flops | bytes accessed | tf_op | source)
XLA Modules:
  0.0 119.0 jit_solution(3797149273505911933)
XLA Ops:
  0.7 0.0 copy-start
  0.7 0.9 copy-done
  1.6 0.0 copy-start.1
  1.6 0.8 copy-done.1
  2.4 0.0 copy-start.2
  2.4 0.8 copy-done.2
  3.2 0.0 copy-start.3
  3.2 0.8 copy-done.3
  4.0 0.0 copy-start.4
  4.0 0.8 copy-done.4
  4.7 0.0 copy-start.5
  4.7 0.8 copy-done.5
  5.5 0.0 copy-start.6
  5.5 0.8 copy-done.6
  6.2 0.0 copy-start.7
  6.2 0.7 copy-done.7
  6.9 0.0 copy-start.8
  6.9 0.7 copy-done.8
  7.6 0.0 copy-start.9
  7.6 0.7 copy-done.9
  8.3 0.0 copy-start.10
  8.3 0.7 copy-done.10
  9.0 0.0 copy-start.11
  9.0 0.7 copy-done.11
  9.7 108.6 %layer.1 = bf16[32,2048]{1,0:T(8,128)(2,1)S(1)} custom-call(f32[1]{0:T(128)S(6)} %copy.16.shift_ref, f32[1,2048]{1,0:T(1,128)S(1)} %bitcast.11, f32[1,2048]{1,0:T(1,128)S(1)} %bitcast.12, f32[1,2048]{1,0:T(1,128)S(1)} %bitcast.13, f32[3,704]{1,0:T(4,128)S(1)} %copy-done.7, f32[3,704]{1,0:T(4,128)S(1)} %copy-done.8, bf16[64,256]{1,0:T(8,128)(2,1)S(1)} %bitcast.8, ...), custom_call_target="tpu_custom_call" | custom-call | tf_op jit(solution)/shard_map/layer/pallas_call | solution.py:527
  118.3 0.7 copy.17
Async XLA Ops:
  0.7 0.9 copy-start
  1.6 0.8 copy-start.1
  2.4 0.8 copy-start.2
  3.2 0.8 copy-start.3
  4.0 0.8 copy-start.4
  4.7 0.8 copy-start.5
  5.5 0.8 copy-start.6
  6.2 0.7 copy-start.7
  6.9 0.7 copy-start.8
  7.6 0.7 copy-start.9
  8.3 0.7 copy-start.10
  9.0 0.7 copy-start.11

commit v3 on v2

--- a/solution.py
+++ b/solution.py
@@ -18,7 +18,7 @@
 HALO = 16
 UNROLL = 4
 TRANSFERS = 256
-LOADS = 8
+LOADS = 14
 
 
 def wrap(v, n):
@@ -48,6 +48,23 @@
             copy.wait_send()
 
 
+class Line:
+    def __init__(self, post, me, place, device):
+        self.post, self.me, self.place, self.device = post, me, place, device
+        self.copies = {}
+
+    def step(self, s):
+        for sign in (1, -1):
+            if (sign, s - 1) in self.copies:
+                self.copies[(sign, s - 1)].wait_recv()
+            if s < RING // 2:
+                part = None if s < RING // 2 - 1 else (0 if sign == 1 else 1)
+                ref = self.place(wrap(self.me - sign * s, RING), part)
+                self.copies[(sign, s)] = self.post.start(
+                    ref, ref, self.device(wrap(self.me + sign, RING))
+                )
+
+
 class Rings:
     def __init__(self, post, z, y, buf):
         self.post, self.z, self.y, self.buf = post, z, y, buf
@@ -79,6 +96,9 @@
             place, place, self._neighbour(h == 1, sign)
         )
 
+    def carries(self, h, sign, c):
+        return sign == -1 if h == 0 else c == (0 if sign == 1 else 1)
+
     def first_step(self, s):
         for h in (0, 1):
             for sign in (1, -1):
@@ -92,7 +112,7 @@
             for sign in (1, -1):
                 if (2, h, sign, s - 1, c) in self.copies:
                     self.copies[(2, h, sign, s - 1, c)].wait_recv()
-                if s < 3 or (s == 3 and c == (0 if sign == 1 else 1)):
+                if s < 3 or (s == 3 and self.carries(h, sign, c)):
                     self.second(h, sign, s, c)
 
 
@@ -129,12 +149,12 @@
 
 
 def layer_kernel(
-    shift_ref,
-    gain_mix,
-    gain_pre,
-    gain_post,
-    conv_gate,
-    conv_up,
+    shift_hbm,
+    mix_hbm,
+    pre_hbm,
+    post_hbm,
+    conv_gate_hbm,
+    conv_up_hbm,
     q_hbm,
     k_hbm,
     v_hbm,
@@ -144,7 +164,13 @@
     resid_hbm,
     wout_hbm,
     result,
-    qt,
+    shift_ref,
+    gain_mix,
+    gain_pre,
+    gain_post,
+    conv_gate,
+    conv_up,
+    queries,
     query,
     pairs,
     gate,
@@ -157,6 +183,9 @@
     acc,
     tail,
     attended,
+    messages,
+    returned,
+    mine,
     arrived,
     piece,
     middle,
@@ -173,6 +202,8 @@
     recv,
     load,
     edge_sem,
+    give_sem,
+    take_sem,
 ):
     sp, tp = lax.axis_index("sp"), lax.axis_index("tp")
     z, y = lax.div(sp, RING), lax.rem(sp, RING)
@@ -188,29 +219,33 @@
         pltpu.make_async_copy(a, b, load.at[i])
         for i, (a, b) in enumerate(
             (
-                (k_hbm, pairs.at[z, y, pl.ds(0, HEAD_DIM)]),
-                (v_hbm, pairs.at[z, y, pl.ds(HEAD_DIM, HEAD_DIM)]),
+                (k_hbm, pairs.at[y, pl.ds(0, HEAD_DIM)]),
+                (v_hbm, pairs.at[y, pl.ds(HEAD_DIM, HEAD_DIM)]),
+                (q_hbm, queries.at[z]),
                 (gate_hbm, gate),
                 (up_hbm, up),
                 (down_hbm, down),
-                (q_hbm, qt),
+                (shift_hbm, shift_ref),
                 (resid_hbm, resid),
                 (wout_hbm, wout),
+                (mix_hbm, gain_mix),
+                (pre_hbm, gain_pre),
+                (post_hbm, gain_post),
+                (conv_gate_hbm, conv_gate),
+                (conv_up_hbm, conv_up),
             )
         )
     ]
     for copy in loads:
         copy.start()
     barrier = pltpu.get_barrier_semaphore()
-    greeted = [
-        {"sp": wrap(z + dz, RING) * RING + wrap(y + dy, RING)}
-        for dz, dy in ((1, 0), (-1, 0), (0, 1), (0, -1))
-    ]
+    greeted = [{"sp": z * RING + wrap(y + k, RING)} for k in (1, -1)]
+    greeted += [{"sp": wrap(z + k, RING) * RING + y} for k in range(1, RING)]
     greeted += [{"sp": wrap(sp + 1, shards)}, {"sp": wrap(sp - 1, shards)}]
     greeted += [{"tp": wrap(tp + k, GROUP)} for k in range(1, GROUP)]
     for device in greeted:
         pl.semaphore_signal(barrier, inc=1, device_id=device, device_id_type=MESH)
-    for copy in loads[2:5]:
+    for copy in loads[3:6]:
         copy.wait()
     for j in range(mains):
         here = slice(j * LANES, (j + 1) * LANES)
@@ -225,89 +260,144 @@
     whole[z, y, :, down_at + mains * LANES :] = jnp.concatenate(
         [down[:, mains * LANES :], jnp.zeros((down.shape[0], LANES - rest), jnp.bfloat16)], axis=1
     )
-    for copy in loads[:2]:
+    for copy in loads[:3]:
         copy.wait()
     pl.semaphore_wait(barrier, len(greeted))
 
     post = Post(send, recv)
-    kv = Rings(post, z, y, pairs)
+
+    def key_place(i, part):
+        return pairs.at[i] if part is None else pairs.at[i, pl.ds(part * HEAD_DIM, HEAD_DIM)]
+
+    def query_place(i, part):
+        half = HEAD_DIM // 2
+        return queries.at[i] if part is None else queries.at[i, pl.ds(part * half, half)]
+
+    kv = Line(post, y, key_place, lambda i: {"sp": z * RING + i})
+    qs = Line(post, z, query_place, lambda i: {"sp": i * RING + y})
     w = Rings(post, z, y, whole)
-    kv.first_step(0)
+    kv.step(0)
+    qs.step(0)
     w.first_step(0)
 
     at = lax.broadcasted_iota(jnp.int32, tri.shape, 0)
     to = lax.broadcasted_iota(jnp.int32, tri.shape, 1)
     tri[...] = jnp.where(at > to, 1.0, 0.0).astype(jnp.bfloat16)
-    loads[5].wait()
-    padded = jnp.concatenate(
-        [qt[...].astype(jnp.float32), jnp.zeros(qt.shape, jnp.float32)], axis=0
-    )
-    query[...] = padded.T.astype(jnp.bfloat16)
+    loads[6].wait()
     shift2 = shift_ref[0] * LOG2E
-    kv.first_step(1)
-    w.first_step(1)
-    first_out, first_tail = tile(query[...], pairs[z, y], tri[...], shift2, True)
-    acc[...] = first_out
-    tail[...] = first_tail
-    for s in (2, 3):
-        kv.first_step(s)
-        w.first_step(s)
-    kv.first_step(4)
-    for c in (0, 1):
-        kv.second_step(0, c)
-    w.first_step(4)
-    for s in (1, 2, 3):
-        for c in (0, 1):
-            kv.second_step(s, c)
-    for c in (0, 1):
-        w.second_step(0, c)
-    for c in (0, 1):
-        kv.second_step(4, c)
-
-    def visit(first, count):
-        found = []
-        for k in range(count):
-            block = sp - first - k
-            pair = pairs[lax.div(block, RING), lax.rem(block, RING)]
-            found.append(tile(query[...], pair, tri[...], shift2, False))
-        total, spent = acc[...], tail[...]
+
+    def set_query(i):
+        padded = jnp.concatenate(
+            [queries[i].astype(jnp.float32), jnp.zeros(queries.shape[1:], jnp.float32)], axis=0
+        )
+        query[...] = padded.T.astype(jnp.bfloat16)
+
+    def visit(first, count, fresh=False):
+        found = [
+            tile(query[...], pairs[first - k], tri[...], shift2, False) for k in range(count)
+        ]
+        if fresh:
+            total, spent = found.pop(0)
+        else:
+            total, spent = acc[...], tail[...]
         for out, more in found:
             total = total + jnp.exp2(-spent) * out
             spent = spent + more
         acc[...] = total
         tail[...] = spent
 
-    odd = lax.rem(sp, UNROLL)
-    many = lax.div(sp, UNROLL)
+    def report():
+        lane = lax.broadcasted_iota(jnp.int32, acc.shape, 1)
+        return jnp.where(lane < HEAD_DIM, tail[...], acc[...]).T
+
+    kv.step(1)
+    qs.step(1)
+    w.first_step(1)
+    set_query(z)
+    first_out, first_tail = tile(query[...], pairs[y], tri[...], shift2, True)
+    acc[...] = first_out
+    tail[...] = first_tail
+    for s in (2, 3):
+        kv.step(s)
+        qs.step(s)
+        w.first_step(s)
+    kv.step(4)
+    qs.step(4)
+    w.first_step(4)
+    for c in (0, 1):
+        w.second_step(0, c)
 
     def one(turn, carry):
-        visit(turn + 1, 1)
+        visit(y - 1 - turn, 1)
         return carry
 
     def several(turn, carry):
-        visit(1 + odd + turn * UNROLL, UNROLL)
+        visit(y - 1 - lax.rem(y, UNROLL) - turn * UNROLL, UNROLL)
         return carry
 
-    lax.fori_loop(0, odd, one, 0)
-    lax.fori_loop(0, jnp.minimum(many, 6), several, 0)
+    lax.fori_loop(0, lax.rem(y, UNROLL), one, 0)
+    lax.fori_loop(0, lax.div(y, UNROLL), several, 0)
+    mine[...] = report()
+
+    def result_copy(i, there):
+        return pltpu.make_async_remote_copy(
+            src_ref=messages.at[i],
+            dst_ref=returned.at[there],
+            send_sem=give_sem.at[i],
+            recv_sem=take_sem.at[there],
+            device_id={"sp": i * RING + y},
+            device_id_type=MESH,
+        )
+
+    def serve(turn, carry):
+        i = z + 1 + turn
+        set_query(i)
+        visit(RING - 1, UNROLL, fresh=True)
+        visit(RING - 1 - UNROLL, UNROLL)
+        found = report()
+        spent = found[: HEAD_DIM // 8, :]
+        high = spent.astype(jnp.bfloat16)
+        low = (spent - high.astype(jnp.float32)).astype(jnp.bfloat16)
+        messages[i] = jnp.concatenate(
+            [found[HEAD_DIM:, :].astype(jnp.bfloat16), high, low], axis=0
+        )
+        result_copy(i, z).start()
+        return carry
+
+    others = RING - 1 - z
+    lax.fori_loop(0, jnp.minimum(others, 3), serve, 0)
     w.second_step(1, 0)
-    lax.fori_loop(6, jnp.minimum(many, 11), several, 0)
+    lax.fori_loop(3, jnp.minimum(others, 5), serve, 0)
     w.second_step(1, 1)
-    lax.fori_loop(11, many, several, 0)
-
-    lane = lax.broadcasted_iota(jnp.int32, acc.shape, 1)
-    mine = lax.div(lane, HEAD_DIM) == core
-    turned = jnp.where(core == 0, pltpu.roll(acc[...], HEAD_DIM, axis=1), acc[...])
-    attended[...] = jnp.where(mine, turned, 0.0).astype(jnp.bfloat16)
+    lax.fori_loop(5, others, serve, 0)
+    w.second_step(2, 0)
+
+    def combine(turn, carry):
+        i = z - 1 - turn
+        result_copy(i, i).wait_recv()
+        spent = mine[:HEAD_DIM, :]
+        low_at = HEAD_DIM + HEAD_DIM // 8
+        more = returned[i, HEAD_DIM : HEAD_DIM + 1, :].astype(jnp.float32)
+        more = more + returned[i, low_at : low_at + 1, :].astype(jnp.float32)
+        mine[HEAD_DIM:, :] += jnp.exp2(-spent) * returned[i, :HEAD_DIM, :].astype(jnp.float32)
+        mine[:HEAD_DIM, :] = spent + more
+        return carry
+
+    lax.fori_loop(0, z, combine, 0)
+    sides = jnp.where(core == 0, 1.0, 0.0)
+    found = mine[HEAD_DIM:, :]
+    attended[...] = jnp.concatenate([found * sides, found * (1.0 - sides)], axis=0).T.astype(
+        jnp.bfloat16
+    )
     exchange = []
     for k in range(1, GROUP):
         peer = wrap(tp + k, GROUP)
         rows = pl.ds(pl.multiple_of(peer * own_rows, own_rows), own_rows)
         exchange.append(post.start(attended.at[rows], arrived.at[tp], {"tp": peer}))
     arrived[tp] = attended[pl.ds(pl.multiple_of(tp * own_rows, own_rows), own_rows), :]
-    w.second_step(2, 0)
-    loads[6].wait()
-    loads[7].wait()
+    w.second_step(2, 1)
+    for copy in loads[7:]:
+        copy.wait()
     for copy in exchange:
         copy.wait_recv()
     heads = jnp.concatenate([arrived[2 * i] + arrived[2 * i + 1] for i in range(CHIPS)], axis=1)
@@ -360,7 +450,6 @@
     def _():
         ahead.start()
 
-    w.second_step(2, 1)
     plus[0].wait_recv()
     plus.append(move(rows_of(left, core, 0), to_chip(right)))
     across.append(move(rows_of(left, core, 0), partner))
@@ -489,6 +578,12 @@
 
     post.drain()
 
+    def sent(turn, carry):
+        result_copy(z + 1 + turn, z).wait_send()
+        return carry
+
+    lax.fori_loop(0, others, sent, 0)
+
     @pl.when(last & (sp < shards - 1))
     def _():
         ahead.wait_send()
@@ -522,17 +617,23 @@
     slab = w_gate.shape[0]
     columns = 2 * mains * LANES + LANES + (mains + 1) * LANES
     vmem = pl.BlockSpec(memory_space=pltpu.VMEM)
-    anywhere = pl.BlockSpec(memory_space=pl.ANY)
+    hbm = pl.BlockSpec(memory_space=pltpu.HBM)
     bf16, f32 = jnp.bfloat16, jnp.float32
     return pl.pallas_call(
         layer_kernel,
         out_shape=jax.ShapeDtypeStruct((own_rows, depth), bf16),
-        in_specs=[pl.BlockSpec(memory_space=pltpu.SMEM)] + [vmem] * 5 + [anywhere] * 8,
+        in_specs=[hbm] * 14,
         out_specs=vmem,
         scratch_shapes=[
-            pltpu.VMEM((HEAD_DIM, span), bf16),
+            pltpu.SMEM((1,), f32),
+            pltpu.VMEM((1, depth), f32),
+            pltpu.VMEM((1, depth), f32),
+            pltpu.VMEM((1, depth), f32),
+            pltpu.VMEM(conv_gate.shape, f32),
+            pltpu.VMEM(conv_up.shape, f32),
+            pltpu.VMEM((RING, HEAD_DIM, span), bf16),
             pltpu.VMEM((span, LANES), bf16),
-            pltpu.VMEM((RING, RING, 2 * HEAD_DIM, span), bf16),
+            pltpu.VMEM((RING, 2 * HEAD_DIM, span), bf16),
             pltpu.VMEM((slab, width), bf16),
             pltpu.VMEM((slab, width), bf16),
             pltpu.VMEM((slab, width), bf16),
@@ -543,6 +644,9 @@
             pltpu.VMEM((span, LANES), f32),
             pltpu.VMEM((span, LANES), f32),
             pltpu.VMEM((span, LANES), bf16),
+            pltpu.VMEM((RING, HEAD_DIM + HEAD_DIM // 4, span), bf16),
+            pltpu.VMEM((RING, HEAD_DIM + HEAD_DIM // 4, span), bf16),
+            pltpu.VMEM((2 * HEAD_DIM, span), f32),
             pltpu.VMEM((GROUP, own_rows, LANES), bf16),
             pltpu.VMEM((HALO + span, depth), bf16),
             pltpu.VMEM((own_rows, depth), f32),
@@ -559,9 +663,11 @@
             pltpu.SemaphoreType.DMA((TRANSFERS,)),
             pltpu.SemaphoreType.DMA((LOADS,)),
             pltpu.SemaphoreType.DMA((GROUP + 1,)),
+            pltpu.SemaphoreType.DMA((RING,)),
+            pltpu.SemaphoreType.DMA((RING,)),
         ],
         compiler_params=pltpu.CompilerParams(
-            collective_id=0, has_side_effects=True, vmem_limit_bytes=52 * 1024 * 1024
+            collective_id=0, has_side_effects=True, vmem_limit_bytes=67_043_328
         ),
         name="layer",
     )(

time: 120 us -> 103 us (0.86)
  Pallas kernels: 109 us -> 99.1 us
  local copies, waits for them, and re-layouts: 9.72 us -> 1.57 us
    pallas_call x1, Pallas kernels: 109 us -> 99.1 us  [local(): pl.pallas_call(layer_kernel, out_shape=jax.ShapeDtypeStruct((own_rows, de...]
    unnamed x25 -> x1, local copies, waits for them, and re-layouts: 9.72 us -> 1.57 us
where the time goes in v3:
time: 103 us; the launch traced here: 101 us
  Pallas kernels  99.1 us (96%)
  local copies, waits for them, and re-layouts  1.57 us (2%)
    pallas_call x1, Pallas kernels, local(): pl.pallas_call(layer_kernel, out_shape=jax.ShapeDtypeStruct((own_rows, de...  99.1 us

profile of v3, /device:TPU:1, one launch (start us, length us, event | category | flops | bytes accessed | tf_op | source)
XLA Modules:
  0.0 101.3 jit_solution(7504031861865950180)
XLA Ops:
  0.7 99.1 %layer.1 = bf16[32,2048]{1,0:T(8,128)(2,1)} custom-call(f32[1]{0:T(128)S(6)} %copy.16.shift_hbm, f32[1,2048]{1,0:T(1,128)} %bitcast.11, f32[1,2048]{1,0:T(1,128)} %bitcast.12, f32[1,2048]{1,0:T(1,128)} %bitcast.13, f32[3,704]{1,0:T(4,128)} %conv_gate_hbm.1, f32[3,704]{1,0:T(4,128)} %conv_up_hbm.1, bf16[64,256]{1,0:T(8,128)(2,1)} %bitcast.8, ...), custom_call_target="tpu_custom_call" | custom-call | tf_op jit(solution)/shard_map/layer/pallas_call | solution.py:622
  99.8 1.6 %copy.17 = bf16[32,2048]{1,0:T(8,128)(2,1)} copy(bf16[32,2048]{1,0:T(8,128)(2,1)} %layer.1) | data formatting | bytes 262144

commit v4 on v3

--- a/solution.py
+++ b/solution.py
@@ -66,10 +66,13 @@
 
 
 class Rings:
+    ORDER = (0, -1, 1, -2, 2, -3, 3, -4)
+
     def __init__(self, post, z, y, buf):
         self.post, self.z, self.y, self.buf = post, z, y, buf
-        rows = buf.shape[2]
-        self.half = (pl.ds(0, rows // 2), pl.ds(rows // 2, rows // 2))
+        tiles = buf.shape[3] // LANES
+        split = tiles // 2 * LANES
+        self.part = (pl.ds(0, split), pl.ds(split, buf.shape[3] - split))
         self.copies = {}
 
     def _neighbour(self, along_y, sign):
@@ -77,27 +80,15 @@
             return {"sp": self.z * RING + wrap(self.y + sign, RING)}
         return {"sp": wrap(self.z + sign, RING) * RING + self.y}
 
-    def first(self, h, sign, s):
-        rows = self.half[h]
+    def _place(self, h, first, second):
         if h == 0:
-            place = self.buf.at[self.z, wrap(self.y - sign * s, RING), rows]
+            z, y = wrap(self.z + second, RING), wrap(self.y + first, RING)
         else:
-            place = self.buf.at[wrap(self.z - sign * s, RING), self.y, rows]
-        self.copies[(1, h, sign, s)] = self.post.start(place, place, self._neighbour(h == 0, sign))
-
-    def second(self, h, sign, s, c):
-        rows = self.half[h]
-        chunk = pl.ds(c * (RING // 2), RING // 2)
-        if h == 0:
-            place = self.buf.at[wrap(self.z - sign * s, RING), chunk, rows]
-        else:
-            place = self.buf.at[chunk, wrap(self.y - sign * s, RING), rows]
-        self.copies[(2, h, sign, s, c)] = self.post.start(
-            place, place, self._neighbour(h == 1, sign)
-        )
-
-    def carries(self, h, sign, c):
-        return sign == -1 if h == 0 else c == (0 if sign == 1 else 1)
+            z, y = wrap(self.z + first, RING), wrap(self.y + second, RING)
+        return self.buf.at[z, y, :, self.part[h]]
+
+    def _carries(self, h, sign, at):
+        return sign == -1 if h == 0 else (at < RING // 2) == (sign == 1)
 
     def first_step(self, s):
         for h in (0, 1):
@@ -105,15 +96,22 @@
                 if (1, h, sign, s - 1) in self.copies:
                     self.copies[(1, h, sign, s - 1)].wait_recv()
                 if s < (4 if sign == 1 else 3):
-                    self.first(h, sign, s)
-
-    def second_step(self, s, c):
-        for h in (0, 1):
-            for sign in (1, -1):
-                if (2, h, sign, s - 1, c) in self.copies:
-                    self.copies[(2, h, sign, s - 1, c)].wait_recv()
-                if s < 3 or (s == 3 and self.carries(h, sign, c)):
-                    self.second(h, sign, s, c)
+                    place = self._place(h, -sign * s, 0)
+                    self.copies[(1, h, sign, s)] = self.post.start(
+                        place, place, self._neighbour(h == 0, sign)
+                    )
+
+    def second_step(self, s, low, high):
+        for at in range(low, high):
+            for h in (0, 1):
+                for sign in (1, -1):
+                    if (2, h, sign, s - 1, at) in self.copies:
+                        self.copies[(2, h, sign, s - 1, at)].wait_recv()
+                    if s < 3 or (s == 3 and self._carries(h, sign, at)):
+                        place = self._place(h, self.ORDER[at], -sign * s)
+                        self.copies[(2, h, sign, s, at)] = self.post.start(
+                            place, place, self._neighbour(h == 1, sign)
+                        )
 
 
 def tile(query, pair, tri, shift2, own):
@@ -279,6 +277,7 @@
     kv.step(0)
     qs.step(0)
     w.first_step(0)
+    w.second_step(0, 0, 1)
 
     at = lax.broadcasted_iota(jnp.int32, tri.shape, 0)
     to = lax.broadcasted_iota(jnp.int32, tri.shape, 1)
@@ -313,6 +312,7 @@
     kv.step(1)
     qs.step(1)
     w.first_step(1)
+    w.second_step(0, 1, 2)
     set_query(z)
     first_out, first_tail = tile(query[...], pairs[y], tri[...], shift2, True)
     acc[...] = first_out
@@ -321,11 +321,11 @@
         kv.step(s)
         qs.step(s)
         w.first_step(s)
+        w.second_step(0, s, s + 1)
     kv.step(4)
     qs.step(4)
     w.first_step(4)
-    for c in (0, 1):
-        w.second_step(0, c)
+    w.second_step(0, 4, 8)
 
     def one(turn, carry):
         visit(y - 1 - turn, 1)
@@ -365,12 +365,12 @@
         return carry
 
     others = RING - 1 - z
-    lax.fori_loop(0, jnp.minimum(others, 3), serve, 0)
-    w.second_step(1, 0)
-    lax.fori_loop(3, jnp.minimum(others, 5), serve, 0)
-    w.second_step(1, 1)
-    lax.fori_loop(5, others, serve, 0)
-    w.second_step(2, 0)
+    lax.fori_loop(0, jnp.minimum(others, 1), serve, 0)
+    w.second_step(1, 0, 4)
+    lax.fori_loop(1, jnp.minimum(others, 4), serve, 0)
+    w.second_step(1, 4, 8)
+    lax.fori_loop(4, others, serve, 0)
+    w.second_step(2, 0, 4)
 
     def combine(turn, carry):
         i = z - 1 - turn
@@ -395,7 +395,7 @@
         rows = pl.ds(pl.multiple_of(peer * own_rows, own_rows), own_rows)
         exchange.append(post.start(attended.at[rows], arrived.at[tp], {"tp": peer}))
     arrived[tp] = attended[pl.ds(pl.multiple_of(tp * own_rows, own_rows), own_rows), :]
-    w.second_step(2, 1)
+    w.second_step(2, 4, 8)
     for copy in loads[7:]:
         copy.wait()
     for copy in exchange:
@@ -450,6 +450,7 @@
     def _():
         ahead.start()
 
+    w.second_step(3, 0, 4)
     plus[0].wait_recv()
     plus.append(move(rows_of(left, core, 0), to_chip(right)))
     across.append(move(rows_of(left, core, 0), partner))
@@ -465,7 +466,6 @@
     across.append(move(rows_of(far, core, 0), partner))
     minus[2].wait_recv()
     across.append(move(rows_of(far, core, 1), partner))
-    w.second_step(3, 0)
 
     spread = [edge_copy(edge_in, {"tp": wrap(tp + k, GROUP)}, k) for k in range(1, GROUP)]
 
@@ -489,9 +489,9 @@
     piece[0:HALO, :] = filled.astype(jnp.bfloat16)
     for copy in across:
         copy.wait_recv()
-    w.second_step(3, 1)
-    w.second_step(4, 0)
-    w.second_step(4, 1)
+    w.second_step(3, 4, 8)
+    w.second_step(4, 0, 4)
+    w.second_step(4, 4, 8)
 
     depth = piece.shape[1]
 
@@ -523,49 +523,64 @@
     inside = lax.broadcasted_iota(jnp.int32, product.shape, 1) < rest
     hidden[:, mains * LANES :] = jnp.where(inside, product, 0.0).astype(jnp.bfloat16)
 
-    for j in range(RING):
-        rhs = whole[j, :, :, down_at:].reshape(depth // RING, hidden.shape[1])
-        found = lax.dot_general(
-            hidden[...], rhs, (((1,), (1,)), ((), ())), preferred_element_type=jnp.float32
-        )
-        partial[:, :, j * (depth // RING) : (j + 1) * (depth // RING)] = found.astype(
-            jnp.bfloat16
-        ).reshape(partial.shape[0], own_rows, depth // RING)
-
-    swaps = [
-        post.start(partial.at[2 * chip + 1 - core], partner_partial.at[chip], partner)
-        for chip in range(CHIPS)
-    ]
+    stripe = depth // RING
+    wide = depth // 2
+    sides_of = [pl.ds(0, wide), pl.ds(wide, wide)]
     halves = (pl.ds(0, own_rows // 2), pl.ds(own_rows // 2, own_rows // 2))
-    for copy in swaps:
-        copy.wait_recv()
-    for chip in range(CHIPS):
-        summed[chip] = (
-            partial[2 * chip + core].astype(jnp.float32)
-            + partner_partial[chip].astype(jnp.float32)
-        ).astype(jnp.bfloat16)
-
-    def give(src, slot, chip):
-        return post.start(src, landed.at[slot], to_chip(chip))
-
-    got = [
-        give(summed.at[far, halves[0]], 0, right),
-        give(summed.at[far, halves[1]], 1, left),
-        give(summed.at[right, halves[1]], 2, right),
-        give(summed.at[left, halves[0]], 3, left),
-    ]
-    got[0].wait_recv()
-    passed[0] = (
-        summed[right, halves[0], :].astype(jnp.float32) + landed[0].astype(jnp.float32)
-    ).astype(jnp.bfloat16)
-    got.append(give(passed.at[0], 4, right))
-    got[1].wait_recv()
-    passed[1] = (
-        summed[left, halves[1], :].astype(jnp.float32) + landed[1].astype(jnp.float32)
-    ).astype(jnp.bfloat16)
-    got.append(give(passed.at[1], 5, left))
-    for copy in got[2:]:
-        copy.wait_recv()
+    swaps = []
+    for part in (0, 1):
+        for j in range(part * RING // 2, (part + 1) * RING // 2):
+            rhs = whole[j, :, :, down_at:].reshape(stripe, hidden.shape[1])
+            found = lax.dot_general(
+                hidden[...], rhs, (((1,), (1,)), ((), ())), preferred_element_type=jnp.float32
+            )
+            partial[:, :, j * stripe : (j + 1) * stripe] = found.astype(jnp.bfloat16).reshape(
+                partial.shape[0], own_rows, stripe
+            )
+        swaps.append(
+            [
+                post.start(
+                    partial.at[2 * chip + 1 - core, :, sides_of[part]],
+                    partner_partial.at[chip, :, sides_of[part]],
+                    partner,
+                )
+                for chip in (far, right, left, x)
+            ]
+        )
+
+    def give(src, slot, part, chip):
+        return post.start(src, landed.at[slot, :, sides_of[part]], to_chip(chip))
+
+    got = []
+    for part in (0, 1):
+        cols = sides_of[part]
+        for copy in swaps[part]:
+            copy.wait_recv()
+        for chip in (far, right, left, x):
+            summed[chip, :, cols] = (
+                partial[2 * chip + core, :, cols].astype(jnp.float32)
+                + partner_partial[chip, :, cols].astype(jnp.float32)
+            ).astype(jnp.bfloat16)
+        got.append(
+            [
+                give(summed.at[far, halves[0], cols], 0, part, right),
+                give(summed.at[far, halves[1], cols], 1, part, left),
+                give(summed.at[right, halves[1], cols], 2, part, right),
+                give(summed.at[left, halves[0], cols], 3, part, left),
+            ]
+        )
+    for part in (0, 1):
+        cols = sides_of[part]
+        for k, (toward, half) in enumerate(((right, 0), (left, 1))):
+            got[part][k].wait_recv()
+            passed[k, :, cols] = (
+                summed[toward, halves[half], cols].astype(jnp.float32)
+                + landed[k, :, cols].astype(jnp.float32)
+            ).astype(jnp.bfloat16)
+            got[part].append(give(passed.at[k, :, cols], 4 + k, part, toward))
+    for part in (0, 1):
+        for copy in got[part][2:]:
+            copy.wait_recv()
     for h, (near, through) in enumerate(((3, 4), (2, 5))):
         ffn = rounded(
             summed[x, halves[h], :].astype(jnp.float32)

time: 103 us -> 96.1 us (0.933); the launches traced: 101 us -> 95.9 us
  Pallas kernels: 99.1 us -> 93.7 us
    pallas_call x1, Pallas kernels: 99.1 us -> 93.7 us  [local(): pl.pallas_call(layer_kernel, out_shape=jax.ShapeDtypeStruct((own_rows, de...]
where the time goes in v4:
time: 96.1 us; the launch traced here: 95.9 us
  Pallas kernels  93.7 us (98%)
  local copies, waits for them, and re-layouts  1.57 us (2%)
    pallas_call x1, Pallas kernels, local(): pl.pallas_call(layer_kernel, out_shape=jax.ShapeDtypeStruct((own_rows, de...  93.7 us

profile of v4, /device:TPU:1, one launch (start us, length us, event | category | flops | bytes accessed | tf_op | source)
XLA Modules:
  0.0 95.9 jit_solution(17123110377477923981)
XLA Ops:
  0.7 93.7 %layer.1 = bf16[32,2048]{1,0:T(8,128)(2,1)} custom-call(f32[1]{0:T(128)S(6)} %copy.16.shift_hbm, f32[1,2048]{1,0:T(1,128)} %bitcast.11, f32[1,2048]{1,0:T(1,128)} %bitcast.12, f32[1,2048]{1,0:T(1,128)} %bitcast.13, f32[3,704]{1,0:T(4,128)} %conv_gate_hbm.1, f32[3,704]{1,0:T(4,128)} %conv_up_hbm.1, bf16[64,256]{1,0:T(8,128)(2,1)} %bitcast.8, ...), custom_call_target="tpu_custom_call" | custom-call | tf_op jit(solution)/shard_map/layer/pallas_call | solution.py:637
  94.4 1.6 %copy.17 = bf16[32,2048]{1,0:T(8,128)(2,1)} copy(bf16[32,2048]{1,0:T(8,128)(2,1)} %layer.1) | data formatting | bytes 262144

commit v5 on v4

--- a/solution.py
+++ b/solution.py
@@ -17,7 +17,8 @@
 LANES = 128
 HALO = 16
 UNROLL = 4
-TRANSFERS = 256
+KINDS = 10
+ARRIVALS = 52
 LOADS = 14
 
 
@@ -27,31 +28,39 @@
 
 class Post:
     def __init__(self, send, recv):
-        self.send, self.recv, self.copies = send, recv, []
-
-    def start(self, src, dst, device):
-        slot = len(self.copies)
-        copy = pltpu.make_async_remote_copy(
-            src_ref=src,
-            dst_ref=dst,
-            send_sem=self.send.at[slot],
-            recv_sem=self.recv.at[slot],
-            device_id=device,
-            device_id_type=MESH,
-        )
-        copy.start()
-        self.copies.append(copy)
-        return copy
-
-    def drain(self):
-        for copy in self.copies:
-            copy.wait_send()
+        self.send, self.recv = send, recv
+        self.kinds, self.slots = 0, 0
+
+    def kind(self):
+        self.kinds += 1
+        return self.send.at[self.kinds - 1]
+
+    def slot(self):
+        self.slots += 1
+        return self.recv.at[self.slots - 1]
+
+
+def remote(src, dst, sent, got, device):
+    return pltpu.make_async_remote_copy(
+        src_ref=src,
+        dst_ref=dst,
+        send_sem=sent,
+        recv_sem=got,
+        device_id=device,
+        device_id_type=MESH,
+    )
+
+
+def started(*arguments):
+    copy = remote(*arguments)
+    copy.start()
+    return copy
 
 
 class Line:
     def __init__(self, post, me, place, device):
         self.post, self.me, self.place, self.device = post, me, place, device
-        self.copies = {}
+        self.sent, self.copies = post.kind(), {}
 
     def step(self, s):
         for sign in (1, -1):
@@ -60,16 +69,20 @@
             if s < RING // 2:
                 part = None if s < RING // 2 - 1 else (0 if sign == 1 else 1)
                 ref = self.place(wrap(self.me - sign * s, RING), part)
-                self.copies[(sign, s)] = self.post.start(
-                    ref, ref, self.device(wrap(self.me + sign, RING))
-                )
+                device = self.device(wrap(self.me + sign, RING))
+                self.copies[(sign, s)] = started(ref, ref, self.sent, self.post.slot(), device)
+
+    def drain(self, whole):
+        device = self.device(wrap(self.me + 1, RING))
+        remote(whole, whole, self.sent, self.sent, device).wait_send()
 
 
 class Rings:
-    ORDER = (0, -1, 1, -2, 2, -3, 3, -4)
-
-    def __init__(self, post, z, y, buf):
-        self.post, self.z, self.y, self.buf = post, z, y, buf
+    STEPS = RING // 2
+
+    def __init__(self, post, z, y, buf, recv):
+        self.post, self.z, self.y, self.buf, self.recv = post, z, y, buf, recv
+        self.sent = [[post.kind() for _ in range(2)] for _ in range(2)]
         tiles = buf.shape[3] // LANES
         split = tiles // 2 * LANES
         self.part = (pl.ds(0, split), pl.ds(split, buf.shape[3] - split))
@@ -87,8 +100,26 @@
             z, y = wrap(self.z + first, RING), wrap(self.y + second, RING)
         return self.buf.at[z, y, :, self.part[h]]
 
-    def _carries(self, h, sign, at):
-        return sign == -1 if h == 0 else (at < RING // 2) == (sign == 1)
+    def _exists(self, h, sign, s, pair):
+        if s < self.STEPS - 1:
+            return True
+        if s > self.STEPS - 1:
+            return False
+        return sign == -1 if h == 0 else (pair < RING // 4) == (sign == 1)
+
+    def _got(self, h, sign, s, pair):
+        return self.recv.at[((2 * h + (sign + 1) // 2) * self.STEPS + s) * (RING // 2) + pair]
+
+    def _second(self, h, sign, s, at):
+        away = jnp.where(lax.rem(at, 2) == 1, -lax.div(at + 1, 2), lax.div(at, 2))
+        place = self._place(h, away, -sign * s)
+        got = self._got(h, sign, s, lax.div(at, 2))
+        return remote(place, place, self.sent[1][h], got, self._neighbour(h == 1, sign))
+
+    def _wait(self, h, sign, s, pair):
+        two = self.buf.at[pl.ds(0, 2), 0, :, self.part[h]]
+        got = self._got(h, sign, s, pair)
+        remote(two, two, self.sent[1][h], got, self._neighbour(h == 1, sign)).wait_recv()
 
     def first_step(self, s):
         for h in (0, 1):
@@ -97,21 +128,51 @@
                     self.copies[(1, h, sign, s - 1)].wait_recv()
                 if s < (4 if sign == 1 else 3):
                     place = self._place(h, -sign * s, 0)
-                    self.copies[(1, h, sign, s)] = self.post.start(
-                        place, place, self._neighbour(h == 0, sign)
+                    device = self._neighbour(h == 0, sign)
+                    self.copies[(1, h, sign, s)] = started(
+                        place, place, self.sent[0][h], self.post.slot(), device
                     )
 
-    def second_step(self, s, low, high):
+    def begin(self, low, high):
         for at in range(low, high):
             for h in (0, 1):
                 for sign in (1, -1):
-                    if (2, h, sign, s - 1, at) in self.copies:
-                        self.copies[(2, h, sign, s - 1, at)].wait_recv()
-                    if s < 3 or (s == 3 and self._carries(h, sign, at)):
-                        place = self._place(h, self.ORDER[at], -sign * s)
-                        self.copies[(2, h, sign, s, at)] = self.post.start(
-                            place, place, self._neighbour(h == 1, sign)
-                        )
+                    self._second(h, sign, 0, jnp.int32(at)).start()
+
+    def forward(self, low, high):
+        def event(n, carry):
+            s, pair = 1 + lax.div(n, RING // 2), lax.rem(n, RING // 2)
+            for h in (0, 1):
+                for sign in (1, -1):
+                    self._wait(h, sign, s - 1, pair)
+                    for k in (0, 1):
+                        self._second(h, sign, s, 2 * pair + k).start()
+            return carry
+
+        lax.fori_loop(low, high, event, 0)
+
+    def last(self, pair):
+        for h in (0, 1):
+            for sign in (1, -1):
+                self._wait(h, sign, self.STEPS - 2, pair)
+                if self._exists(h, sign, self.STEPS - 1, pair):
+                    for k in (0, 1):
+                        self._second(h, sign, self.STEPS - 1, jnp.int32(2 * pair + k)).start()
+
+    def finish(self):
+        for h in (0, 1):
+            for sign in (1, -1):
+                for pair in range(RING // 2):
+                    if self._exists(h, sign, self.STEPS - 1, pair):
+                        self._wait(h, sign, self.STEPS - 1, pair)
+
+    def drain(self):
+        for h in (0, 1):
+            once = self.buf.at[0, pl.ds(0, RING - 1), :, self.part[h]]
+            rows = self.buf.at[pl.ds(0, RING - 1), :, :, self.part[h]]
+            for phase, moved in enumerate((once, rows)):
+                sent = self.sent[phase][h]
+                remote(moved, moved, sent, sent, self._neighbour(True, 1)).wait_send()
 
 
 def tile(query, pair, tri, shift2, own):
@@ -202,6 +263,8 @@
     edge_sem,
     give_sem,
     take_sem,
+    ring_recv,
+    early,
 ):
     sp, tp = lax.axis_index("sp"), lax.axis_index("tp")
     z, y = lax.div(sp, RING), lax.rem(sp, RING)
@@ -273,11 +336,11 @@
 
     kv = Line(post, y, key_place, lambda i: {"sp": z * RING + i})
     qs = Line(post, z, query_place, lambda i: {"sp": i * RING + y})
-    w = Rings(post, z, y, whole)
+    w = Rings(post, z, y, whole, ring_recv)
     kv.step(0)
     qs.step(0)
     w.first_step(0)
-    w.second_step(0, 0, 1)
+    w.begin(0, 1)
 
     at = lax.broadcasted_iota(jnp.int32, tri.shape, 0)
     to = lax.broadcasted_iota(jnp.int32, tri.shape, 1)
@@ -312,7 +375,7 @@
     kv.step(1)
     qs.step(1)
     w.first_step(1)
-    w.second_step(0, 1, 2)
+    w.begin(1, 2)
     set_query(z)
     first_out, first_tail = tile(query[...], pairs[y], tri[...], shift2, True)
     acc[...] = first_out
@@ -321,11 +384,11 @@
         kv.step(s)
         qs.step(s)
         w.first_step(s)
-        w.second_step(0, s, s + 1)
+        w.begin(s, s + 1)
     kv.step(4)
     qs.step(4)
     w.first_step(4)
-    w.second_step(0, 4, 8)
+    w.begin(4, 8)
 
     def one(turn, carry):
         visit(y - 1 - turn, 1)
@@ -365,12 +428,18 @@
         return carry
 
     others = RING - 1 - z
-    lax.fori_loop(0, jnp.minimum(others, 1), serve, 0)
-    w.second_step(1, 0, 4)
-    lax.fori_loop(1, jnp.minimum(others, 4), serve, 0)
-    w.second_step(1, 4, 8)
-    lax.fori_loop(4, others, serve, 0)
-    w.second_step(2, 0, 4)
+
+    def paced(turn):
+        return 1 + lax.div(3 * turn, 4)
+
+    def serve_and_forward(turn, carry):
+        serve(turn, carry)
+        w.forward(paced(turn), paced(turn + 1))
+        return carry
+
+    w.forward(0, 1)
+    lax.fori_loop(0, others, serve_and_forward, 0)
+    w.forward(paced(others), 7)
 
     def combine(turn, carry):
         i = z - 1 - turn
@@ -389,17 +458,17 @@
     attended[...] = jnp.concatenate([found * sides, found * (1.0 - sides)], axis=0).T.astype(
         jnp.bfloat16
     )
-    exchange = []
+    swapped, pieces_in = post.kind(), post.slot()
     for k in range(1, GROUP):
         peer = wrap(tp + k, GROUP)
         rows = pl.ds(pl.multiple_of(peer * own_rows, own_rows), own_rows)
-        exchange.append(post.start(attended.at[rows], arrived.at[tp], {"tp": peer}))
+        started(attended.at[rows], arrived.at[tp], swapped, pieces_in, {"tp": peer})
     arrived[tp] = attended[pl.ds(pl.multiple_of(tp * own_rows, own_rows), own_rows), :]
-    w.second_step(2, 4, 8)
+    w.forward(7, 8)
     for copy in loads[7:]:
         copy.wait()
-    for copy in exchange:
-        copy.wait_recv()
+    pieces = arrived.at[pl.ds(0, GROUP - 1)]
+    remote(pieces, pieces, swapped, pieces_in, {"tp": wrap(tp + 1, GROUP)}).wait_recv()
     heads = jnp.concatenate([arrived[2 * i] + arrived[2 * i + 1] for i in range(CHIPS)], axis=1)
     mixed = rounded(jnp.dot(heads, wout[...], preferred_element_type=jnp.float32))
     mid = rounded(resid[...].astype(jnp.float32) + gain_mix[...] * rms_scale(mixed))
@@ -420,8 +489,13 @@
 
     partner = {"tp": 2 * x + 1 - core}
 
+    spread_out, crossed = post.kind(), post.slot()
+
     def move(ref, device):
-        return post.start(ref, ref, device)
+        return started(ref, ref, spread_out, post.slot(), device)
+
+    def cross(ref):
+        started(ref, ref, spread_out, crossed, partner)
 
     piece[pl.ds(pl.multiple_of(HALO + tp * own_rows, HALO), own_rows), :] = normed.astype(
         jnp.bfloat16
@@ -431,7 +505,7 @@
     minus = [move(rows_of(x, core, 1), to_chip(left))]
     plus.append(move(rows_of(x, core, 1), to_chip(right)))
     minus.append(move(rows_of(x, core, 0), to_chip(left)))
-    across = [move(rows_of(x, core), partner)]
+    cross(rows_of(x, core))
 
     def edge_copy(src, device, slot):
         return pltpu.make_async_remote_copy(
@@ -450,22 +524,25 @@
     def _():
         ahead.start()
 
-    w.second_step(3, 0, 4)
+    w.last(0)
     plus[0].wait_recv()
     plus.append(move(rows_of(left, core, 0), to_chip(right)))
-    across.append(move(rows_of(left, core, 0), partner))
+    cross(rows_of(left, core, 0))
+    w.last(1)
     minus[0].wait_recv()
     minus.append(move(rows_of(right, core, 1), to_chip(left)))
-    across.append(move(rows_of(right, core, 1), partner))
+    cross(rows_of(right, core, 1))
+    w.last(2)
     plus[1].wait_recv()
-    across.append(move(rows_of(left, core, 1), partner))
+    cross(rows_of(left, core, 1))
     minus[1].wait_recv()
-    across.append(move(rows_of(right, core, 0), partner))
+    cross(rows_of(right, core, 0))
+    w.last(3)
     far = wrap(x + 2, CHIPS)
     plus[2].wait_recv()
-    across.append(move(rows_of(far, core, 0), partner))
+    cross(rows_of(far, core, 0))
     minus[2].wait_recv()
-    across.append(move(rows_of(far, core, 1), partner))
+    cross(rows_of(far, core, 1))
 
     spread = [edge_copy(edge_in, {"tp": wrap(tp + k, GROUP)}, k) for k in range(1, GROUP)]
 
@@ -487,13 +564,22 @@
         jnp.where((place == HALO - 2) & (front == 1), behind[0:1, :], 0.0),
     )
     piece[0:HALO, :] = filled.astype(jnp.bfloat16)
-    for copy in across:
-        copy.wait_recv()
-    w.second_step(3, 4, 8)
-    w.second_step(4, 0, 4)
-    w.second_step(4, 4, 8)
-
+    crossings = piece.at[pl.ds(0, GROUP // 2 * own_rows)]
+    remote(crossings, crossings, spread_out, crossed, partner).wait_recv()
     depth = piece.shape[1]
+    stripe = depth // RING
+    ready = (2 * mains + 1 + mains + 1) // 2 // 2
+    for j in range(ready):
+        found = 0.0
+        for d in range(1 - RING // 2, RING // 2):
+            near = wrap(z + d, RING)
+            found = found + jnp.dot(
+                piece[:, pl.ds(pl.multiple_of(near * stripe, stripe), stripe)],
+                whole[near, :, :, 2 * j * LANES : (2 * j + 2) * LANES].reshape(stripe, 2 * LANES),
+                preferred_element_type=jnp.float32,
+            )
+        early[j] = found
+    w.finish()
 
     def convolve(low, high, taps):
         rows = partial.shape[0] * own_rows
@@ -509,8 +595,17 @@
 
     for j in range(mains):
         cols = slice(2 * j * LANES, (2 * j + 2) * LANES)
-        rhs = whole[:, :, :, cols].reshape(depth, 2 * LANES)
-        extended[...] = rounded(jnp.dot(piece[...], rhs, preferred_element_type=jnp.float32))
+        if j < ready:
+            opposite = wrap(z + RING // 2, RING)
+            found = early[j] + jnp.dot(
+                piece[:, pl.ds(pl.multiple_of(opposite * stripe, stripe), stripe)],
+                whole[opposite, :, :, cols].reshape(stripe, 2 * LANES),
+                preferred_element_type=jnp.float32,
+            )
+        else:
+            rhs = whole[:, :, :, cols].reshape(depth, 2 * LANES)
+            found = jnp.dot(piece[...], rhs, preferred_element_type=jnp.float32)
+        extended[...] = rounded(found)
         here = slice(j * LANES, (j + 1) * LANES)
         g = convolve(0, LANES, conv_gate[:, here])
         u = convolve(LANES, 2 * LANES, conv_up[:, here])
@@ -523,11 +618,11 @@
     inside = lax.broadcasted_iota(jnp.int32, product.shape, 1) < rest
     hidden[:, mains * LANES :] = jnp.where(inside, product, 0.0).astype(jnp.bfloat16)
 
-    stripe = depth // RING
     wide = depth // 2
     sides_of = [pl.ds(0, wide), pl.ds(wide, wide)]
     halves = (pl.ds(0, own_rows // 2), pl.ds(own_rows // 2, own_rows // 2))
-    swaps = []
+    halved, summing = post.kind(), post.kind()
+    swap_in = [post.slot(), post.slot()]
     for part in (0, 1):
         for j in range(part * RING // 2, (part + 1) * RING // 2):
             rhs = whole[j, :, :, down_at:].reshape(stripe, hidden.shape[1])
@@ -537,25 +632,24 @@
             partial[:, :, j * stripe : (j + 1) * stripe] = found.astype(jnp.bfloat16).reshape(
                 partial.shape[0], own_rows, stripe
             )
-        swaps.append(
-            [
-                post.start(
-                    partial.at[2 * chip + 1 - core, :, sides_of[part]],
-                    partner_partial.at[chip, :, sides_of[part]],
-                    partner,
-                )
-                for chip in (far, right, left, x)
-            ]
-        )
+        for chip in range(CHIPS):
+            started(
+                partial.at[2 * chip + 1 - core, :, sides_of[part]],
+                partner_partial.at[chip, :, sides_of[part]],
+                halved,
+                swap_in[part],
+                partner,
+            )
 
     def give(src, slot, part, chip):
-        return post.start(src, landed.at[slot, :, sides_of[part]], to_chip(chip))
+        there = landed.at[slot, :, sides_of[part]]
+        return started(src, there, summing, post.slot(), to_chip(chip))
 
     got = []
     for part in (0, 1):
         cols = sides_of[part]
-        for copy in swaps[part]:
-            copy.wait_recv()
+        swaps = partner_partial.at[:, :, cols]
+        remote(swaps, swaps, halved, swap_in[part], partner).wait_recv()
         for chip in (far, right, left, x):
             summed[chip, :, cols] = (
                 partial[2 * chip + core, :, cols].astype(jnp.float32)
@@ -569,6 +663,18 @@
                 give(summed.at[left, halves[0], cols], 3, part, left),
             ]
         )
+    kv.drain(pairs.at[pl.ds(0, RING - 1)])
+    qs.drain(queries.at[pl.ds(0, RING - 1)])
+    w.drain()
+    remote(pieces, pieces, swapped, swapped, partner).wait_send()
+    moved = piece.at[pl.ds(0, (GROUP - 1) * own_rows)]
+    remote(moved, moved, spread_out, spread_out, partner).wait_send()
+
+    def sent(turn, carry):
+        result_copy(z + 1 + turn, z).wait_send()
+        return carry
+
+    lax.fori_loop(0, others, sent, 0)
     for part in (0, 1):
         cols = sides_of[part]
         for k, (toward, half) in enumerate(((right, 0), (left, 1))):
@@ -591,13 +697,8 @@
             middle[halves[h], :] + gain_post[...] * rms_scale(ffn)
         ).astype(jnp.bfloat16)
 
-    post.drain()
-
-    def sent(turn, carry):
-        result_copy(z + 1 + turn, z).wait_send()
-        return carry
-
-    lax.fori_loop(0, others, sent, 0)
+    remote(partner_partial, partner_partial, halved, halved, partner).wait_send()
+    remote(landed, landed, summing, summing, partner).wait_send()
 
     @pl.when(last & (sp < shards - 1))
     def _():
@@ -674,12 +775,14 @@
             pltpu.VMEM((CHIPS, own_rows, depth), bf16),
             pltpu.VMEM((6, own_rows // 2, depth), bf16),
             pltpu.VMEM((2, own_rows // 2, depth), bf16),
-            pltpu.SemaphoreType.DMA((TRANSFERS,)),
-            pltpu.SemaphoreType.DMA((TRANSFERS,)),
+            pltpu.SemaphoreType.DMA((KINDS,)),
+            pltpu.SemaphoreType.DMA((ARRIVALS,)),
             pltpu.SemaphoreType.DMA((LOADS,)),
             pltpu.SemaphoreType.DMA((GROUP + 1,)),
             pltpu.SemaphoreType.DMA((RING,)),
             pltpu.SemaphoreType.DMA((RING,)),
+            pltpu.SemaphoreType.DMA((RING * RING,)),
+            pltpu.VMEM((CHIPS, HALO + span, 2 * LANES), f32),
         ],
         compiler_params=pltpu.CompilerParams(
             collective_id=0, has_side_effects=True, vmem_limit_bytes=67_043_328

time: 96.1 us -> 91.4 us (0.951)
  Pallas kernels: 93.7 us -> 89 us
    pallas_call x1, Pallas kernels: 93.7 us -> 89 us  [local(): pl.pallas_call(layer_kernel, out_shape=jax.ShapeDtypeStruct((own_rows, de...]
where the time goes in v5:
time: 91.4 us; the launch traced here: 91.2 us
  Pallas kernels  89 us (97%)
  local copies, waits for them, and re-layouts  1.57 us (2%)
    pallas_call x1, Pallas kernels, local(): pl.pallas_call(layer_kernel, out_shape=jax.ShapeDtypeStruct((own_rows, de...  89 us

profile of v5, /device:TPU:1, one launch (start us, length us, event | category | flops | bytes accessed | tf_op | source)
XLA Modules:
  0.0 91.2 jit_solution(8834746371833250539)
XLA Ops:
  0.7 89.0 %layer.1 = bf16[32,2048]{1,0:T(8,128)(2,1)} custom-call(f32[1]{0:T(128)S(6)} %copy.16.shift_hbm, f32[1,2048]{1,0:T(1,128)} %bitcast.11, f32[1,2048]{1,0:T(1,128)} %bitcast.12, f32[1,2048]{1,0:T(1,128)} %bitcast.13, f32[3,704]{1,0:T(4,128)} %conv_gate_hbm.1, f32[3,704]{1,0:T(4,128)} %conv_up_hbm.1, bf16[64,256]{1,0:T(8,128)(2,1)} %bitcast.8, ...), custom_call_target="tpu_custom_call" | custom-call | tf_op jit(solution)/shard_map/layer/pallas_call | solution.py:738
  89.6 1.6 %copy.17 = bf16[32,2048]{1,0:T(8,128)(2,1)} copy(bf16[32,2048]{1,0:T(8,128)(2,1)} %layer.1) | data formatting | bytes 262144

commit v6 on v5

--- a/solution.py
+++ b/solution.py
@@ -18,7 +18,7 @@
 HALO = 16
 UNROLL = 4
 KINDS = 10
-ARRIVALS = 52
+ARRIVALS = 45
 LOADS = 14
 
 
@@ -80,12 +80,9 @@
 class Rings:
     STEPS = RING // 2
 
-    def __init__(self, post, z, y, buf, recv):
-        self.post, self.z, self.y, self.buf, self.recv = post, z, y, buf, recv
+    def __init__(self, post, z, y, bufs, recv):
+        self.post, self.z, self.y, self.bufs, self.recv = post, z, y, bufs, recv
         self.sent = [[post.kind() for _ in range(2)] for _ in range(2)]
-        tiles = buf.shape[3] // LANES
-        split = tiles // 2 * LANES
-        self.part = (pl.ds(0, split), pl.ds(split, buf.shape[3] - split))
         self.copies = {}
 
     def _neighbour(self, along_y, sign):
@@ -98,14 +95,14 @@
             z, y = wrap(self.z + second, RING), wrap(self.y + first, RING)
         else:
             z, y = wrap(self.z + first, RING), wrap(self.y + second, RING)
-        return self.buf.at[z, y, :, self.part[h]]
+        return self.bufs[h].at[z, y]
 
     def _exists(self, h, sign, s, pair):
         if s < self.STEPS - 1:
             return True
         if s > self.STEPS - 1:
             return False
-        return sign == -1 if h == 0 else (pair < RING // 4) == (sign == 1)
+        return (pair < RING // 4) == (sign == 1)
 
     def _got(self, h, sign, s, pair):
         return self.recv.at[((2 * h + (sign + 1) // 2) * self.STEPS + s) * (RING // 2) + pair]
@@ -117,7 +114,7 @@
         return remote(place, place, self.sent[1][h], got, self._neighbour(h == 1, sign))
 
     def _wait(self, h, sign, s, pair):
-        two = self.buf.at[pl.ds(0, 2), 0, :, self.part[h]]
+        two = self.bufs[h].at[pl.ds(0, 2), 0]
         got = self._got(h, sign, s, pair)
         remote(two, two, self.sent[1][h], got, self._neighbour(h == 1, sign)).wait_recv()
 
@@ -159,17 +156,16 @@
                     for k in (0, 1):
                         self._second(h, sign, self.STEPS - 1, jnp.int32(2 * pair + k)).start()
 
-    def finish(self):
-        for h in (0, 1):
-            for sign in (1, -1):
-                for pair in range(RING // 2):
-                    if self._exists(h, sign, self.STEPS - 1, pair):
-                        self._wait(h, sign, self.STEPS - 1, pair)
+    def finish(self, h):
+        for sign in (1, -1):
+            for pair in range(RING // 2):
+                if self._exists(h, sign, self.STEPS - 1, pair):
+                    self._wait(h, sign, self.STEPS - 1, pair)
 
     def drain(self):
         for h in (0, 1):
-            once = self.buf.at[0, pl.ds(0, RING - 1), :, self.part[h]]
-            rows = self.buf.at[pl.ds(0, RING - 1), :, :, self.part[h]]
+            once = self.bufs[h].at[0, pl.ds(0, RING - 1)]
+            rows = self.bufs[h].at[pl.ds(0, RING - 1)]
             for phase, moved in enumerate((once, rows)):
                 sent = self.sent[phase][h]
                 remote(moved, moved, sent, sent, self._neighbour(True, 1)).wait_send()
@@ -235,7 +231,8 @@
     gate,
     up,
     down,
-    whole,
+    early_blocks,
+    late_blocks,
     resid,
     wout,
     tri,
@@ -297,8 +294,6 @@
             )
         )
     ]
-    for copy in loads:
-        copy.start()
     barrier = pltpu.get_barrier_semaphore()
     greeted = [{"sp": z * RING + wrap(y + k, RING)} for k in (1, -1)]
     greeted += [{"sp": wrap(z + k, RING) * RING + y} for k in range(1, RING)]
@@ -306,23 +301,32 @@
     greeted += [{"tp": wrap(tp + k, GROUP)} for k in range(1, GROUP)]
     for device in greeted:
         pl.semaphore_signal(barrier, inc=1, device_id=device, device_id_type=MESH)
-    for copy in loads[3:6]:
+    for copy in loads:
+        copy.start()
+    for copy in loads[:6]:
         copy.wait()
-    for j in range(mains):
+    slab = gate.shape[0]
+
+    def columns(j):
         here = slice(j * LANES, (j + 1) * LANES)
-        whole[z, y, :, 2 * j * LANES : (2 * j + 1) * LANES] = gate[:, here]
-        whole[z, y, :, (2 * j + 1) * LANES : (2 * j + 2) * LANES] = up[:, here]
-    base = 2 * mains * LANES
-    whole[z, y, :, base : base + LANES] = jnp.concatenate(
-        [gate[:, mains * LANES :], up[:, mains * LANES :]], axis=1
+        return [gate[:, here], up[:, here]]
+
+    ends = jnp.concatenate([gate[:, mains * LANES :], up[:, mains * LANES :]], axis=1)
+    ready = early_blocks.shape[2] // slab // 2
+    for j in range(ready):
+        for k, block in enumerate(columns(j)):
+            at = (2 * j + k) * slab
+            early_blocks[z, y, at : at + slab] = block
+    later_blocks = [block for j in range(ready, mains) for block in columns(j)] + [ends]
+    down_at = len(later_blocks)
+    later_blocks += [down[:, j * LANES : (j + 1) * LANES] for j in range(mains)]
+    for k, block in enumerate(later_blocks):
+        late_blocks[z, y, k * slab : (k + 1) * slab] = block
+    half = slab // 2
+    end = down[:, mains * LANES :]
+    late_blocks[z, y, len(later_blocks) * slab :] = jnp.concatenate(
+        [end[:half], end[half:]], axis=1
     )
-    down_at = base + LANES
-    whole[z, y, :, down_at : down_at + mains * LANES] = down[:, : mains * LANES]
-    whole[z, y, :, down_at + mains * LANES :] = jnp.concatenate(
-        [down[:, mains * LANES :], jnp.zeros((down.shape[0], LANES - rest), jnp.bfloat16)], axis=1
-    )
-    for copy in loads[:3]:
-        copy.wait()
     pl.semaphore_wait(barrier, len(greeted))
 
     post = Post(send, recv)
@@ -336,7 +340,7 @@
 
     kv = Line(post, y, key_place, lambda i: {"sp": z * RING + i})
     qs = Line(post, z, query_place, lambda i: {"sp": i * RING + y})
-    w = Rings(post, z, y, whole, ring_recv)
+    w = Rings(post, z, y, (early_blocks, late_blocks), ring_recv)
     kv.step(0)
     qs.step(0)
     w.first_step(0)
@@ -413,7 +417,7 @@
         )
 
     def serve(turn, carry):
-        i = z + 1 + turn
+        i = RING - 1 - turn
         set_query(i)
         visit(RING - 1, UNROLL, fresh=True)
         visit(RING - 1 - UNROLL, UNROLL)
@@ -430,14 +434,13 @@
     others = RING - 1 - z
 
     def paced(turn):
-        return 1 + lax.div(3 * turn, 4)
+        return lax.div(3 * turn, 4)
 
     def serve_and_forward(turn, carry):
         serve(turn, carry)
         w.forward(paced(turn), paced(turn + 1))
         return carry
 
-    w.forward(0, 1)
     lax.fori_loop(0, others, serve_and_forward, 0)
     w.forward(paced(others), 7)
 
@@ -568,18 +571,28 @@
     remote(crossings, crossings, spread_out, crossed, partner).wait_recv()
     depth = piece.shape[1]
     stripe = depth // RING
-    ready = (2 * mains + 1 + mains + 1) // 2 // 2
+
+    def slabs(blocks, where, k):
+        found = blocks[where, :, k * slab : (k + 1) * slab]
+        return found.reshape(RING * slab, LANES)
+
+    def all_slabs(k):
+        return late_blocks[:, :, k * slab : (k + 1) * slab].reshape(RING * RING * slab, LANES)
+
+    def pair_product(where, j):
+        rhs = jnp.concatenate(
+            [slabs(early_blocks, where, 2 * j), slabs(early_blocks, where, 2 * j + 1)], axis=1
+        )
+        lhs = piece[:, pl.ds(pl.multiple_of(where * stripe, stripe), stripe)]
+        return jnp.dot(lhs, rhs, preferred_element_type=jnp.float32)
+
     for j in range(ready):
         found = 0.0
         for d in range(1 - RING // 2, RING // 2):
-            near = wrap(z + d, RING)
-            found = found + jnp.dot(
-                piece[:, pl.ds(pl.multiple_of(near * stripe, stripe), stripe)],
-                whole[near, :, :, 2 * j * LANES : (2 * j + 2) * LANES].reshape(stripe, 2 * LANES),
-                preferred_element_type=jnp.float32,
-            )
+            found = found + pair_product(wrap(z + d, RING), j)
         early[j] = found
-    w.finish()
+    w.finish(1)
+    w.finish(0)
 
     def convolve(low, high, taps):
         rows = partial.shape[0] * own_rows
@@ -594,24 +607,21 @@
         return v / (1.0 + jnp.exp(-v))
 
     for j in range(mains):
-        cols = slice(2 * j * LANES, (2 * j + 2) * LANES)
         if j < ready:
-            opposite = wrap(z + RING // 2, RING)
-            found = early[j] + jnp.dot(
-                piece[:, pl.ds(pl.multiple_of(opposite * stripe, stripe), stripe)],
-                whole[opposite, :, :, cols].reshape(stripe, 2 * LANES),
-                preferred_element_type=jnp.float32,
-            )
+            found = early[j] + pair_product(wrap(z + RING // 2, RING), j)
         else:
-            rhs = whole[:, :, :, cols].reshape(depth, 2 * LANES)
+            k = 2 * (j - ready)
+            rhs = jnp.concatenate([all_slabs(k), all_slabs(k + 1)], axis=1)
             found = jnp.dot(piece[...], rhs, preferred_element_type=jnp.float32)
         extended[...] = rounded(found)
         here = slice(j * LANES, (j + 1) * LANES)
         g = convolve(0, LANES, conv_gate[:, here])
         u = convolve(LANES, 2 * LANES, conv_up[:, here])
         hidden[:, here] = (silu(g) * u).astype(jnp.bfloat16)
-    rhs = whole[:, :, :, base : base + LANES].reshape(depth, LANES)
-    extended[:, :LANES] = rounded(jnp.dot(piece[...], rhs, preferred_element_type=jnp.float32))
+    found = jnp.dot(
+        piece[...], all_slabs(2 * (mains - ready)), preferred_element_type=jnp.float32
+    )
+    extended[:, :LANES] = rounded(found)
     taps = jnp.concatenate([conv_gate[:, mains * LANES :], conv_up[:, mains * LANES :]], axis=1)
     both = convolve(0, LANES, taps)
     product = silu(both) * pltpu.roll(both, LANES - rest, axis=1)
@@ -625,7 +635,18 @@
     swap_in = [post.slot(), post.slot()]
     for part in (0, 1):
         for j in range(part * RING // 2, (part + 1) * RING // 2):
-            rhs = whole[j, :, :, down_at:].reshape(stripe, hidden.shape[1])
+            end = late_blocks[j, :, len(later_blocks) * slab :].astype(jnp.float32)
+            end = end.reshape(RING * half, LANES)
+            inside = lax.broadcasted_iota(jnp.int32, end.shape, 1) < rest
+            ends = [
+                jnp.where(inside, v, 0.0).astype(jnp.bfloat16).reshape(RING, half, LANES)
+                for v in (end, pltpu.roll(end, LANES - rest, axis=1))
+            ]
+            rhs = jnp.concatenate(
+                [slabs(late_blocks, j, down_at + k) for k in range(mains)]
+                + [jnp.concatenate(ends, axis=1).reshape(stripe, LANES)],
+                axis=1,
+            )
             found = lax.dot_general(
                 hidden[...], rhs, (((1,), (1,)), ((), ())), preferred_element_type=jnp.float32
             )
@@ -641,9 +662,12 @@
                 partner,
             )
 
+    ends_in = post.slot()
+
     def give(src, slot, part, chip):
         there = landed.at[slot, :, sides_of[part]]
-        return started(src, there, summing, post.slot(), to_chip(chip))
+        arrival = post.slot() if slot < 2 else ends_in
+        return started(src, there, summing, arrival, to_chip(chip))
 
     got = []
     for part in (0, 1):
@@ -683,10 +707,9 @@
                 summed[toward, halves[half], cols].astype(jnp.float32)
                 + landed[k, :, cols].astype(jnp.float32)
             ).astype(jnp.bfloat16)
-            got[part].append(give(passed.at[k, :, cols], 4 + k, part, toward))
-    for part in (0, 1):
-        for copy in got[part][2:]:
-            copy.wait_recv()
+            give(passed.at[k, :, cols], 4 + k, part, toward)
+    ending = landed.at[pl.ds(2, 4)]
+    remote(ending, ending, summing, ends_in, partner).wait_recv()
     for h, (near, through) in enumerate(((3, 4), (2, 5))):
         ffn = rounded(
             summed[x, halves[h], :].astype(jnp.float32)
@@ -731,7 +754,8 @@
     width = w_gate.shape[1]
     mains = width // LANES
     slab = w_gate.shape[0]
-    columns = 2 * mains * LANES + LANES + (mains + 1) * LANES
+    tiles = 3 * mains + 1
+    early_tiles = tiles // 4 * 2
     vmem = pl.BlockSpec(memory_space=pltpu.VMEM)
     hbm = pl.BlockSpec(memory_space=pltpu.HBM)
     bf16, f32 = jnp.bfloat16, jnp.float32
@@ -753,7 +777,8 @@
             pltpu.VMEM((slab, width), bf16),
             pltpu.VMEM((slab, width), bf16),
             pltpu.VMEM((slab, width), bf16),
-            pltpu.VMEM((RING, RING, slab, columns), bf16),
+            pltpu.VMEM((RING, RING, early_tiles * slab, LANES), bf16),
+            pltpu.VMEM((RING, RING, (tiles - early_tiles) * slab + slab // 2, LANES), bf16),
             pltpu.VMEM((own_rows, depth), bf16),
             pltpu.VMEM(w_out.shape, bf16),
             pltpu.VMEM((span, span), bf16),
@@ -782,7 +807,7 @@
             pltpu.SemaphoreType.DMA((RING,)),
             pltpu.SemaphoreType.DMA((RING,)),
             pltpu.SemaphoreType.DMA((RING * RING,)),
-            pltpu.VMEM((CHIPS, HALO + span, 2 * LANES), f32),
+            pltpu.VMEM((early_tiles // 2, HALO + span, 2 * LANES), f32),
         ],
         compiler_params=pltpu.CompilerParams(
             collective_id=0, has_side_effects=True, vmem_limit_bytes=67_043_328

time: 91.4 us -> 85.9 us (0.940)
  Pallas kernels: 89 us -> 83.2 us
    pallas_call x1, Pallas kernels: 89 us -> 83.2 us  [local(): pl.pallas_call(layer_kernel, out_shape=jax.ShapeDtypeStruct((own_rows, de...]
where the time goes in v6:
time: 85.9 us; the launch traced here: 85.4 us
  Pallas kernels  83.2 us (97%)
  local copies, waits for them, and re-layouts  1.57 us (2%)
    pallas_call x1, Pallas kernels, local(): pl.pallas_call(layer_kernel, out_shape=jax.ShapeDtypeStruct((own_rows, de...  83.2 us

profile of v6, /device:TPU:1, one launch (start us, length us, event | category | flops | bytes accessed | tf_op | source)
XLA Modules:
  0.0 85.4 jit_solution(3969466110930165936)
XLA Ops:
  0.7 83.2 %layer.1 = bf16[32,2048]{1,0:T(8,128)(2,1)} custom-call(f32[1]{0:T(128)S(6)} %copy.16.shift_hbm, f32[1,2048]{1,0:T(1,128)} %bitcast.11, f32[1,2048]{1,0:T(1,128)} %bitcast.12, f32[1,2048]{1,0:T(1,128)} %bitcast.13, f32[3,704]{1,0:T(4,128)} %conv_gate_hbm.1, f32[3,704]{1,0:T(4,128)} %conv_up_hbm.1, bf16[64,256]{1,0:T(8,128)(2,1)} %bitcast.8, ...), custom_call_target="tpu_custom_call" | custom-call | tf_op jit(solution)/shard_map/layer/pallas_call | solution.py:762
  83.8 1.6 %copy.17 = bf16[32,2048]{1,0:T(8,128)(2,1)} copy(bf16[32,2048]{1,0:T(8,128)(2,1)} %layer.1) | data formatting | bytes 262144

commit v7 on v6

--- a/solution.py
+++ b/solution.py
@@ -18,7 +18,7 @@
 HALO = 16
 UNROLL = 4
 KINDS = 10
-ARRIVALS = 45
+ARRIVALS = 31
 LOADS = 14
 
 
@@ -58,32 +58,38 @@
 
 
 class Line:
-    def __init__(self, post, me, place, device):
-        self.post, self.me, self.place, self.device = post, me, place, device
-        self.sent, self.copies = post.kind(), {}
+    STEPS = RING // 2
+
+    def __init__(self, post, me, buf, place, device):
+        self.me, self.buf, self.place, self.device = me, buf, place, device
+        self.sent = post.kind()
+        self.got = [post.slot() for _ in range(self.STEPS)]
+
+    def _settle(self, ref, got):
+        return remote(ref, ref, self.sent, got, self.device(wrap(self.me + 1, RING)))
 
     def step(self, s):
-        for sign in (1, -1):
-            if (sign, s - 1) in self.copies:
-                self.copies[(sign, s - 1)].wait_recv()
-            if s < RING // 2:
-                part = None if s < RING // 2 - 1 else (0 if sign == 1 else 1)
+        if s > 0:
+            count = 2 if s < self.STEPS else 1
+            self._settle(self.buf.at[pl.ds(0, count)], self.got[s - 1]).wait_recv()
+        if s < self.STEPS:
+            for sign in (1, -1):
+                part = None if s < self.STEPS - 1 else (0 if sign == 1 else 1)
                 ref = self.place(wrap(self.me - sign * s, RING), part)
                 device = self.device(wrap(self.me + sign, RING))
-                self.copies[(sign, s)] = started(ref, ref, self.sent, self.post.slot(), device)
-
-    def drain(self, whole):
-        device = self.device(wrap(self.me + 1, RING))
-        remote(whole, whole, self.sent, self.sent, device).wait_send()
+                started(ref, ref, self.sent, self.got[s], device)
+
+    def drain(self):
+        self._settle(self.buf.at[pl.ds(0, RING - 1)], self.sent).wait_send()
 
 
 class Rings:
     STEPS = RING // 2
 
     def __init__(self, post, z, y, bufs, recv):
-        self.post, self.z, self.y, self.bufs, self.recv = post, z, y, bufs, recv
+        self.z, self.y, self.bufs, self.recv = z, y, bufs, recv
         self.sent = [[post.kind() for _ in range(2)] for _ in range(2)]
-        self.copies = {}
+        self.got = [[post.slot() for _ in range(self.STEPS)] for _ in range(2)]
 
     def _neighbour(self, along_y, sign):
         if along_y:
@@ -97,38 +103,31 @@
             z, y = wrap(self.z + first, RING), wrap(self.y + second, RING)
         return self.bufs[h].at[z, y]
 
-    def _exists(self, h, sign, s, pair):
-        if s < self.STEPS - 1:
-            return True
-        if s > self.STEPS - 1:
-            return False
-        return (pair < RING // 4) == (sign == 1)
-
-    def _got(self, h, sign, s, pair):
-        return self.recv.at[((2 * h + (sign + 1) // 2) * self.STEPS + s) * (RING // 2) + pair]
+    def _got(self, h, s, pair):
+        return self.recv.at[(h * self.STEPS + s) * (RING // 2) + pair]
 
     def _second(self, h, sign, s, at):
         away = jnp.where(lax.rem(at, 2) == 1, -lax.div(at + 1, 2), lax.div(at, 2))
         place = self._place(h, away, -sign * s)
-        got = self._got(h, sign, s, lax.div(at, 2))
+        got = self._got(h, s, lax.div(at, 2))
         return remote(place, place, self.sent[1][h], got, self._neighbour(h == 1, sign))
 
-    def _wait(self, h, sign, s, pair):
-        two = self.bufs[h].at[pl.ds(0, 2), 0]
-        got = self._got(h, sign, s, pair)
-        remote(two, two, self.sent[1][h], got, self._neighbour(h == 1, sign)).wait_recv()
+    def _wait(self, h, s, pair, sides=2):
+        blocks = self.bufs[h].at[pl.ds(0, 2 * sides), 0]
+        got = self._got(h, s, pair)
+        remote(blocks, blocks, self.sent[1][h], got, self._neighbour(h == 1, 1)).wait_recv()
 
     def first_step(self, s):
         for h in (0, 1):
+            if s > 0:
+                blocks = self.bufs[h].at[0, pl.ds(0, 2 if s < self.STEPS else 1)]
+                device = self._neighbour(h == 0, 1)
+                remote(blocks, blocks, self.sent[0][h], self.got[h][s - 1], device).wait_recv()
             for sign in (1, -1):
-                if (1, h, sign, s - 1) in self.copies:
-                    self.copies[(1, h, sign, s - 1)].wait_recv()
-                if s < (4 if sign == 1 else 3):
+                if s < (self.STEPS if sign == 1 else self.STEPS - 1):
                     place = self._place(h, -sign * s, 0)
                     device = self._neighbour(h == 0, sign)
-                    self.copies[(1, h, sign, s)] = started(
-                        place, place, self.sent[0][h], self.post.slot(), device
-                    )
+                    started(place, place, self.sent[0][h], self.got[h][s], device)
 
     def begin(self, low, high):
         for at in range(low, high):
@@ -140,27 +139,24 @@
         def event(n, carry):
             s, pair = 1 + lax.div(n, RING // 2), lax.rem(n, RING // 2)
             for h in (0, 1):
-                for sign in (1, -1):
-                    self._wait(h, sign, s - 1, pair)
-                    for k in (0, 1):
+                self._wait(h, s - 1, pair)
+                for k in (0, 1):
+                    for sign in (1, -1):
                         self._second(h, sign, s, 2 * pair + k).start()
             return carry
 
         lax.fori_loop(low, high, event, 0)
 
     def last(self, pair):
+        sign = 1 if pair < RING // 4 else -1
         for h in (0, 1):
-            for sign in (1, -1):
-                self._wait(h, sign, self.STEPS - 2, pair)
-                if self._exists(h, sign, self.STEPS - 1, pair):
-                    for k in (0, 1):
-                        self._second(h, sign, self.STEPS - 1, jnp.int32(2 * pair + k)).start()
+            self._wait(h, self.STEPS - 2, pair)
+            for k in (0, 1):
+                self._second(h, sign, self.STEPS - 1, jnp.int32(2 * pair + k)).start()
 
     def finish(self, h):
-        for sign in (1, -1):
-            for pair in range(RING // 2):
-                if self._exists(h, sign, self.STEPS - 1, pair):
-                    self._wait(h, sign, self.STEPS - 1, pair)
+        for pair in range(RING // 2):
+            self._wait(h, self.STEPS - 1, pair, 1)
 
     def drain(self):
         for h in (0, 1):
@@ -338,8 +334,8 @@
         half = HEAD_DIM // 2
         return queries.at[i] if part is None else queries.at[i, pl.ds(part * half, half)]
 
-    kv = Line(post, y, key_place, lambda i: {"sp": z * RING + i})
-    qs = Line(post, z, query_place, lambda i: {"sp": i * RING + y})
+    kv = Line(post, y, pairs, key_place, lambda i: {"sp": z * RING + i})
+    qs = Line(post, z, queries, query_place, lambda i: {"sp": i * RING + y})
     w = Rings(post, z, y, (early_blocks, late_blocks), ring_recv)
     kv.step(0)
     qs.step(0)
@@ -419,8 +415,7 @@
     def serve(turn, carry):
         i = RING - 1 - turn
         set_query(i)
-        visit(RING - 1, UNROLL, fresh=True)
-        visit(RING - 1 - UNROLL, UNROLL)
+        visit(RING - 1, RING, fresh=True)
         found = report()
         spent = found[: HEAD_DIM // 8, :]
         high = spent.astype(jnp.bfloat16)
@@ -592,7 +587,6 @@
             found = found + pair_product(wrap(z + d, RING), j)
         early[j] = found
     w.finish(1)
-    w.finish(0)
 
     def convolve(low, high, taps):
         rows = partial.shape[0] * own_rows
@@ -606,18 +600,17 @@
     def silu(v):
         return v / (1.0 + jnp.exp(-v))
 
-    for j in range(mains):
-        if j < ready:
-            found = early[j] + pair_product(wrap(z + RING // 2, RING), j)
-        else:
-            k = 2 * (j - ready)
-            rhs = jnp.concatenate([all_slabs(k), all_slabs(k + 1)], axis=1)
-            found = jnp.dot(piece[...], rhs, preferred_element_type=jnp.float32)
+    def gated(j, found):
         extended[...] = rounded(found)
         here = slice(j * LANES, (j + 1) * LANES)
         g = convolve(0, LANES, conv_gate[:, here])
         u = convolve(LANES, 2 * LANES, conv_up[:, here])
         hidden[:, here] = (silu(g) * u).astype(jnp.bfloat16)
+
+    for j in range(ready, mains):
+        k = 2 * (j - ready)
+        rhs = jnp.concatenate([all_slabs(k), all_slabs(k + 1)], axis=1)
+        gated(j, jnp.dot(piece[...], rhs, preferred_element_type=jnp.float32))
     found = jnp.dot(
         piece[...], all_slabs(2 * (mains - ready)), preferred_element_type=jnp.float32
     )
@@ -627,6 +620,9 @@
     product = silu(both) * pltpu.roll(both, LANES - rest, axis=1)
     inside = lax.broadcasted_iota(jnp.int32, product.shape, 1) < rest
     hidden[:, mains * LANES :] = jnp.where(inside, product, 0.0).astype(jnp.bfloat16)
+    w.finish(0)
+    for j in range(ready):
+        gated(j, early[j] + pair_product(wrap(z + RING // 2, RING), j))
 
     wide = depth // 2
     sides_of = [pl.ds(0, wide), pl.ds(wide, wide)]
@@ -687,8 +683,8 @@
                 give(summed.at[left, halves[0], cols], 3, part, left),
             ]
         )
-    kv.drain(pairs.at[pl.ds(0, RING - 1)])
-    qs.drain(queries.at[pl.ds(0, RING - 1)])
+    kv.drain()
+    qs.drain()
     w.drain()
     remote(pieces, pieces, swapped, swapped, partner).wait_send()
     moved = piece.at[pl.ds(0, (GROUP - 1) * own_rows)]
@@ -806,7 +802,7 @@
             pltpu.SemaphoreType.DMA((GROUP + 1,)),
             pltpu.SemaphoreType.DMA((RING,)),
             pltpu.SemaphoreType.DMA((RING,)),
-            pltpu.SemaphoreType.DMA((RING * RING,)),
+            pltpu.SemaphoreType.DMA((RING * RING // 2,)),
             pltpu.VMEM((early_tiles // 2, HALO + span, 2 * LANES), f32),
         ],
         compiler_params=pltpu.CompilerParams(

time: 85.9 us -> 86.1 us (level)
  no operation moved by 1% of the time
where the time goes in v7:
time: 86.1 us; the launch traced here: 85.9 us
  Pallas kernels  83.7 us (97%)
  local copies, waits for them, and re-layouts  1.57 us (2%)
    pallas_call x1, Pallas kernels, local(): pl.pallas_call(layer_kernel, out_shape=jax.ShapeDtypeStruct((own_rows, de...  83.7 us

profile of v7, /device:TPU:1, one launch (start us, length us, event | category | flops | bytes accessed | tf_op | source)
XLA Modules:
  0.0 85.9 jit_solution(16397866520862900867)
XLA Ops:
  0.7 83.7 %layer.1 = bf16[32,2048]{1,0:T(8,128)(2,1)} custom-call(f32[1]{0:T(128)S(6)} %copy.16.shift_hbm, f32[1,2048]{1,0:T(1,128)} %bitcast.11, f32[1,2048]{1,0:T(1,128)} %bitcast.12, f32[1,2048]{1,0:T(1,128)} %bitcast.13, f32[3,704]{1,0:T(4,128)} %conv_gate_hbm.1, f32[3,704]{1,0:T(4,128)} %conv_up_hbm.1, bf16[64,256]{1,0:T(8,128)(2,1)} %bitcast.8, ...), custom_call_target="tpu_custom_call" | custom-call | tf_op jit(solution)/shard_map/layer/pallas_call | solution.py:758
  84.4 1.6 %copy.17 = bf16[32,2048]{1,0:T(8,128)(2,1)} copy(bf16[32,2048]{1,0:T(8,128)(2,1)} %layer.1) | data formatting | bytes 262144
